TPU v7x, 512 devices: a whole 4x8x8 slice. The times are simulated.
512 devices in a mesh: sp: 32 (over z, x), tp: 16 (over y, core).
Axes of the slice: x: 4, y: 8, z: 8, core: 2. Of those that a mesh axis runs over, the one named last changes fastest.
Arguments:
- moe_input: bfloat16 [4096, 2048], P('sp'), may hold values from -6 to 6
- out_grad: bfloat16 [4096, 2048], P('sp'), may hold values from -6 to 6
- routes: int32 [4096, 2], P('sp'), may hold values from 0 to 31, all different within a row; in each aligned block of 128 rows (0 to 127, 128 to 255, ...) at most 10 rows name the same one
- route_weight: float32 [4096, 2], P('sp'), may hold values from 0.2 to 1.2
- w_gate: bfloat16 [32, 2048, 2048], P('sp', None, 'tp'), may hold values from -0.125 to 0.125
- w_up: bfloat16 [32, 2048, 2048], P('sp', None, 'tp'), may hold values from -0.125 to 0.125
- w_down: bfloat16 [32, 2048, 2048], P('sp', 'tp'), may hold values from -0.125 to 0.125
- w_out: bfloat16 [2048, 4096], P(None, 'tp'), may hold values from -0.09375 to 0.09375
- query_heads: bfloat16 [16, 4096, 128], P('tp', 'sp'), may hold values from -6 to 6
- key_heads: bfloat16 [16, 4096, 128], P('tp', 'sp'), may hold values from -6 to 6
- value_heads: bfloat16 [16, 4096, 256], P('tp', 'sp'), may hold values from -6 to 6
- log_decay: float32 [16, 4096], P('tp', 'sp'), may hold values from -0.6 to 0
- state_in: float32 [16, 32, 128, 256], P('tp', 'sp'), may hold values from -4 to 4
Outputs:
- gate_grad: bfloat16 [32, 2048, 2048], P('sp', None, 'tp')
- up_grad: bfloat16 [32, 2048, 2048], P('sp', None, 'tp')
- down_grad: bfloat16 [32, 2048, 2048], P('sp', 'tp')
- out_proj_grad: float32 [2048, 4096], P('sp', 'tp')
- query_gradient: bfloat16 [16, 4096, 128], P('tp', 'sp')
- key_grad: bfloat16 [16, 4096, 128], P('tp', 'sp')
- value_grad: bfloat16 [16, 4096, 256], P('tp', 'sp')
Inputs may be any that keep to these rules, and one draw needn't show every extreme that they name: `routes`: each row names 2 different experts; within each aligned block of 128 tokens no expert is named more than 10 times, and exactly 10 times for some expert in some blocks.
All inputs are finite; a program needn't handle non-finite values.
Results may differ from a plain program's by a relative error of at most 0.025.
Values may be sent and summed in bfloat16 or wider, within the bound.
A program may use at most 64 MiB of HBM per device.

v0:
```python
import jax
import jax.numpy as jnp
from jax import lax
from jax.sharding import Mesh
from jax.sharding import PartitionSpec as P

BLOCK = 64
SP = ("sp_0", "sp_1")


def sent_together(arrays, axis, split_dim, concat_dim, along):
    widths = [a.shape[along] for a in arrays]
    both = jnp.concatenate(arrays, axis=along)
    whole = lax.all_to_all(both, axis, split_axis=split_dim, concat_axis=concat_dim, tiled=True)
    return tuple(jnp.split(whole, [sum(widths[:k]) for k in range(1, len(widths))], axis=along))


def in_one_piece(arrays, axis, dim, along):
    widths = [a.shape[along] for a in arrays]
    both = jnp.concatenate(arrays, axis=along)
    whole = lax.all_gather(both, axis, axis=dim, tiled=True)
    return tuple(jnp.split(whole, [sum(widths[:k]) for k in range(1, len(widths))], axis=along))


def neutral_like(shard, identity):
    return jax.tree.map(
        lambda a, e: jnp.broadcast_to(jnp.asarray(e, a.dtype), a.shape), shard, identity
    )


def prefix_by_axis(shard, axes, combine, identity):
    before = start = neutral_like(shard, identity)
    subtotal = shard
    for axis in reversed(axes):
        length, position = (lax.axis_size(axis), lax.axis_index(axis))
        pieces = jax.tree.map(
            lambda part, kind: lax.all_gather(part.astype(kind), axis),
            subtotal,
            (jnp.bfloat16, jnp.bfloat16),
        )
        inside, subtotal = (start, start)
        for k in reversed(range(length)):
            passed = k > position
            subtotal = combine(
                subtotal, jax.tree.map(lambda part, own: part[k].astype(own.dtype), pieces, shard)
            )
            inside = jax.tree.map(lambda new, old: jnp.where(passed, new, old), subtotal, inside)
        before = combine(inside, before)
    return before


def cut_along(shard, dim, length):
    lengths = shard.shape
    pieces = shard.reshape(*lengths[:dim], length, lengths[dim] // length, *lengths[dim + 1 :])
    return jnp.moveaxis(pieces, dim, 0)


def summed_on_arrival(shard, axis, dim):
    pieces = cut_along(shard, dim, lax.axis_size(axis))
    arrived = lax.all_to_all(pieces, axis, split_axis=0, concat_axis=0, tiled=True)
    return arrived.astype(jnp.float32).sum(axis=0)


def silu_slope(gate_pre):
    sigmoid_v = jax.nn.sigmoid(gate_pre)
    return sigmoid_v * (1.0 + gate_pre * (1.0 - sigmoid_v))


def decay_table(log_sums):
    block_size = log_sums.shape[-1]
    token_positions = jnp.arange(block_size)
    lower_mask = (token_positions[:, None] >= token_positions[None, :])[None]
    log_diff = jnp.where(lower_mask, log_sums[:, :, None] - log_sums[:, None, :], 0.0)
    return jnp.where(lower_mask, jnp.exp(log_diff), 0.0)


def forward_block(forwarded_state, inputs):
    query_rows, rescaled_keys, value_rows, head_gradients, log_sums = inputs
    decay_mat = decay_table(log_sums)
    scores = jnp.einsum("htk,hsk->hts", query_rows, rescaled_keys) * decay_mat
    leading_decay = jnp.exp(log_sums)[:, :, None]
    trailing_decay = jnp.exp(log_sums[:, -1:] - log_sums)[:, :, None]
    blended_heads = jnp.einsum("hts,hsv->htv", scores, value_rows)
    blended_heads = blended_heads + jnp.einsum(
        "imj,iju->imu", query_rows * leading_decay, forwarded_state
    )
    back_scores = jnp.einsum("htv,hsv->hts", head_gradients, value_rows) * decay_mat
    query_gradient = jnp.einsum("hts,hsk->htk", back_scores, rescaled_keys)
    query_gradient = query_gradient + jnp.einsum(
        "fqg,fug->fqu", head_gradients * leading_decay, forwarded_state
    )
    forwarded_state = jnp.exp(log_sums[:, -1])[:, None, None] * forwarded_state + jnp.einsum(
        "nbq,nbc->nqc", rescaled_keys * trailing_decay, value_rows
    )
    return (forwarded_state, (blended_heads, query_gradient))


def reverse_block(forwarded_state, inputs):
    query_rows, rescaled_keys, value_rows, head_gradients, log_sums = inputs
    decay_mat = decay_table(log_sums)
    scores = jnp.einsum("htk,hsk->hts", query_rows, rescaled_keys) * decay_mat
    back_scores = jnp.einsum("htv,hsv->hts", head_gradients, value_rows) * decay_mat
    leading_decay = jnp.exp(log_sums)[:, :, None]
    trailing_decay = jnp.exp(log_sums[:, -1:] - log_sums)[:, :, None]
    key_portion = jnp.einsum("hts,htk->hsk", back_scores, query_rows)
    key_portion = key_portion + jnp.einsum(
        "lbg,ljg->lbj", value_rows * trailing_decay, forwarded_state
    )
    value_portion = jnp.einsum("hts,htv->hsv", scores, head_gradients)
    value_portion = value_portion + jnp.einsum(
        "bea,baz->bez", rescaled_keys * trailing_decay, forwarded_state
    )
    forwarded_state = jnp.exp(log_sums[:, -1])[:, None, None] * forwarded_state + jnp.einsum(
        "byj,byg->bjg", query_rows * leading_decay, head_gradients
    )
    return (forwarded_state, (key_portion, value_portion))


def link_states(higher_part, lower_part):
    return (
        higher_part[0] * lower_part[0],
        lower_part[1] + lower_part[0][:, None, None] * higher_part[1],
    )


def expert_backward(rows_in, grad_in, w_gate, w_up, w_down):
    gate_pre = jnp.einsum("erd,edf->erf", rows_in, w_gate, preferred_element_type=jnp.float32)
    up_pre = jnp.einsum("erd,edf->erf", rows_in, w_up, preferred_element_type=jnp.float32)
    active = jax.nn.silu(gate_pre)
    hidden = (active * up_pre).astype(jnp.bfloat16)
    hidden_back = jnp.einsum("erd,efd->erf", grad_in, w_down, preferred_element_type=jnp.float32)
    down_part = jnp.einsum("erf,erd->efd", hidden, grad_in, preferred_element_type=jnp.float32)
    gate_back = (hidden_back * up_pre * silu_slope(gate_pre)).astype(jnp.bfloat16)
    up_back = (hidden_back * active).astype(jnp.bfloat16)
    gate_part = jnp.einsum("erd,erf->edf", rows_in, gate_back, preferred_element_type=jnp.float32)
    up_part = jnp.einsum("erd,erf->edf", rows_in, up_back, preferred_element_type=jnp.float32)
    partial_value = jnp.einsum(
        "erf,edf->erd", gate_back, w_gate, preferred_element_type=jnp.float32
    )
    partial_value = partial_value + jnp.einsum(
        "erf,edf->erd", up_back, w_up, preferred_element_type=jnp.float32
    )
    return (
        gate_part.astype(jnp.bfloat16),
        up_part.astype(jnp.bfloat16),
        down_part.astype(jnp.bfloat16),
        partial_value.astype(jnp.bfloat16),
    )


def body(
    moe_input,
    out_grad,
    routes,
    route_weight,
    w_gate,
    w_up,
    w_down,
    w_out,
    query_heads,
    key_heads,
    value_heads,
    log_decay,
    state_in,
):
    tok_rows, model_width = moe_input.shape
    picks = routes.shape[1]
    experts = w_gate.shape[0] * lax.axis_size(SP)
    capacity = 5 * tok_rows * picks // (4 * experts)
    route_ids = routes.reshape(-1)
    routed = route_ids.shape[0]
    onehot = (route_ids[:, None] == jnp.arange(experts, dtype=jnp.int32)[None, :]).astype(jnp.int32)
    slot_index = jnp.sum(jnp.cumsum(onehot, axis=0) * onehot, axis=1) - 1
    target = route_ids * capacity + slot_index
    source = (
        jnp.full((experts * capacity,), routed, jnp.int32)
        .at[target]
        .set(jnp.arange(routed, dtype=jnp.int32))
    )
    filled = source < routed
    picked = jnp.where(filled, source, 0)
    token_idx = picked // picks
    weight_slot = jnp.where(filled, route_weight.reshape(-1)[picked], 0.0)
    send_rows = jnp.where(filled[:, None], moe_input[token_idx], jnp.zeros((), jnp.bfloat16))
    send_rows = send_rows.reshape(experts, capacity, model_width)
    send_grad = (weight_slot[:, None] * out_grad[token_idx].astype(jnp.float32)).astype(
        jnp.bfloat16
    )
    send_grad = send_grad.reshape(experts, capacity, model_width)
    group_count = lax.axis_size("tp")
    slice_width = model_width // group_count
    offset = lax.axis_index("tp") * slice_width
    pieces = (
        lax.dynamic_slice_in_dim(send_rows, offset, slice_width, 2),
        lax.dynamic_slice_in_dim(send_grad, offset, slice_width, 2),
    )
    pieces = sent_together((pieces[0], pieces[1]), SP, 0, 1, 2)
    rows_in, grad_in = in_one_piece((pieces[0], pieces[1]), "tp", 2, 0)
    gate_grad, up_grad, down_grad, partial_value = expert_backward(
        rows_in, grad_in, w_gate, w_up, w_down
    )
    local_rows = partial_value.shape[1]
    grouped = partial_value.reshape(partial_value.shape[0], local_rows, group_count, slice_width)
    spread_parts = lax.all_to_all(grouped, "tp", split_axis=2, concat_axis=2, tiled=True)
    feature_part = jnp.sum(spread_parts.astype(jnp.float32), axis=2).astype(jnp.bfloat16)
    returned_part = lax.all_to_all(feature_part, SP, split_axis=1, concat_axis=0, tiled=True)
    returned = lax.all_gather(returned_part, "tp", axis=2, tiled=True)
    gathered = returned.reshape(experts * capacity, model_width)[target].reshape(
        tok_rows, picks, model_width
    )
    mixed_grad = (
        out_grad.astype(jnp.float32) + jnp.sum(gathered.astype(jnp.float32), axis=1)
    ).astype(jnp.bfloat16)
    head_count = query_heads.shape[0]
    key_size = key_heads.shape[-1]
    value_size = value_heads.shape[-1]
    head_grad = jnp.dot(mixed_grad, w_out, preferred_element_type=jnp.float32).astype(jnp.bfloat16)
    head_gradients = (
        head_grad.reshape(tok_rows, head_count, value_size).transpose(1, 0, 2).astype(jnp.float32)
    )
    query_rows = query_heads.astype(jnp.float32)
    rescaled_keys = key_heads.astype(jnp.float32) * key_size ** (-0.5)
    value_rows = value_heads.astype(jnp.float32)
    block_count = tok_rows // BLOCK

    def to_blocks(array):
        return array.reshape(head_count, block_count, BLOCK, array.shape[-1]).transpose(1, 0, 2, 3)

    def from_blocks(array):
        return array.transpose(1, 0, 2, 3).reshape(head_count, tok_rows, array.shape[-1])

    log_sums = jnp.cumsum(log_decay.reshape(head_count, block_count, BLOCK), axis=2).transpose(
        1, 0, 2
    )
    inputs = (
        to_blocks(query_rows),
        to_blocks(rescaled_keys),
        to_blocks(value_rows),
        to_blocks(head_gradients),
        log_sums,
    )
    _, (blended_heads, query_gradient) = lax.scan(forward_block, state_in[:, 0], inputs)
    running_total = jnp.cumsum(log_decay, axis=1)
    carried = jnp.einsum(
        "byj,byg->bjg", query_rows * jnp.exp(running_total)[:, :, None], head_gradients
    )
    span_keep = jnp.exp(running_total[:, -1])
    incoming = prefix_by_axis(
        (span_keep, carried), SP, link_states, (jnp.ones_like(span_keep), jnp.zeros_like(carried))
    )[1]
    _, (key_grad, value_grad) = lax.scan(reverse_block, incoming, inputs, reverse=True)
    mixed_flat = (
        from_blocks(blended_heads)
        .astype(jnp.bfloat16)
        .transpose(1, 0, 2)
        .reshape(tok_rows, head_count * value_size)
    )
    out_proj_grad = summed_on_arrival(
        lax.dot_general(
            mixed_grad, mixed_flat, (((0,), (0,)), ((), ())), preferred_element_type=jnp.float32
        ).astype(jnp.bfloat16),
        SP,
        0,
    )
    query_gradient = from_blocks(query_gradient).astype(jnp.bfloat16)
    key_grad = (from_blocks(key_grad) * key_size ** (-0.5)).astype(jnp.bfloat16)
    value_grad = from_blocks(value_grad).astype(jnp.bfloat16)
    return (gate_grad, up_grad, down_grad, out_proj_grad, query_gradient, key_grad, value_grad)


def solution(mesh):
    finer = Mesh(mesh.devices.reshape(8, 4, mesh.shape["tp"]), ("sp_0", "sp_1", "tp"))
    return jax.shard_map(
        body,
        mesh=finer,
        in_specs=(
            P(SP, None),
            P(SP, None),
            P(SP, None),
            P(SP, None),
            P(SP, None, "tp"),
            P(SP, None, "tp"),
            P(SP, "tp", None),
            P(None, "tp"),
            P("tp", SP, None),
            P("tp", SP, None),
            P("tp", SP, None),
            P("tp", SP),
            P("tp", SP, None, None),
        ),
        out_specs=(
            P(SP, None, "tp"),
            P(SP, None, "tp"),
            P(SP, "tp", None),
            P(SP, "tp"),
            P("tp", SP, None),
            P("tp", SP, None),
            P("tp", SP, None),
        ),
        check_vma=False,
    )
```

profile of v0, /device:TPU:6, one launch (start us, length us, event | category | flops | bytes accessed | tf_op | source)
XLA Modules:
  0.0 296.1 jit_solution(285302291044372434)
XLA Ops:
  7.2 0.8 broadcast_multiply_fusion
  8.0 0.8 copy.41
  9.4 0.6 reduce-window.6
  10.3 1.4 scatter_custom_fusion
  11.9 2.4 gather_fusion.2
  14.4 2.1 reshape.1008
  16.7 2.5 gather_fusion.1
  19.3 2.4 gather_fusion
  21.8 1.6 gather.15
  23.3 1.1 fusion.134
  24.4 1.1 dynamic-slice_select_fusion
  25.6 24.4 %all_to_all.34 = bf16[32,10,256]{2,1,0:T(8,128)(2,1)S(1)} all-to-all(bf16[32,10,256]{2,1,0:T(8,128)(2,1)S(1)} %pad_maximum_fusion), channel_id=1, replica_groups=mesh['sp_0'=8,'sp_1'=4,'tp'=16] {'sp_0','sp_1'}, dimensions={0} | all-to-all | bytes 327680 | tf_op jit(solution)/shard_map/all_to_all | solution.py:14
  50.1 0.7 pad_maximum_fusion.1
  50.9 41.8 %all-gather.5.cloned.1.call-done = bf16[2,320,2048]{2,1,0:T(8,128)(2,1)} async-done(((bf16[2,320,128]{2,1,0:T(8,128)(2,1)}), bf16[2,320,2048]{2,1,0:T(8,128)(2,1)}) %all-gather.5.cloned.1.call-update) | async-done | bytes 2621456 | tf_op jit(solution)/shard_map/all_gather | solution.py:21
  92.7 2.0 fusion.126
  94.7 1.9 fusion.127
  96.6 0.5 multiply_convert_fusion.1
  97.1 0.5 fusion.128
  97.7 0.5 fusion.124
  98.9 38.4 %all_to_all.35 = bf16[1,320,16,128]{3,1,0,2:T(8,128)(2,1)S(1)} all-to-all(bf16[1,320,16,128]{3,1,0,2:T(8,128)(2,1)S(1)} %copy.45), channel_id=1, replica_groups=mesh['sp_0'=8,'sp_1'=4,'tp'=16] {'tp'}, dimensions={2} | all-to-all | bytes 2621440 | tf_op jit(solution)/shard_map/all_to_all | solution.py:204
  137.6 0.5 broadcast.599
  138.2 1.1 reduce.10
  139.3 19.3 %all_to_all.36 = bf16[32,2,640]{2,1,0:T(2,128)(2,1)S(1)} all-to-all(bf16[32,2,640]{2,1,0:T(2,128)(2,1)S(1)} %reshape.1204), channel_id=1, replica_groups=mesh['sp_0'=8,'sp_1'=4,'tp'=16] {'sp_0','sp_1'}, dimensions={0} | all-to-all | bytes 163840 | tf_op jit(solution)/shard_map/all_to_all | solution.py:206
  158.7 0.5 bitcast_reduce_fusion
  159.2 0.7 all_to_all.28
  160.2 0.6 slice.98
  161.5 1.3 dynamic-slice
  162.8 0.8 dynamic-update-slice
  163.5 8.3 %all-reduce = bf16[4]{0:T(256)(128)(2,1)S(1)} all-reduce(bf16[4]{0:T(256)(128)(2,1)S(1)} %dynamic-update-slice), channel_id=1, replica_groups=mesh['sp_0'=8,'sp_1'=4,'tp'=16] {'sp_1'}, use_global_device_ids=true, to_apply=%add | all-reduce | flops 4 | bytes 16
  171.8 1.3 dynamic-slice.1
  173.1 0.6 fusion.166
  173.7 1.4 dynamic-update-slice.1
  175.1 15.2 %all-reduce.1 = bf16[8]{0:T(256)(128)(2,1)S(1)} all-reduce(bf16[8]{0:T(256)(128)(2,1)S(1)} %dynamic-update-slice.1), channel_id=3, replica_groups=mesh['sp_0'=8,'sp_1'=4,'tp'=16] {'sp_0'}, use_global_device_ids=true, to_apply=%add.1 | all-reduce | flops 8 | bytes 32
  190.3 0.5 broadcast.595
  190.9 0.7 reduce.8
  191.6 0.7 fusion.165
  196.1 0.6 slice_convert_fusion
  198.6 0.5 reduce_window_sum.42
  201.7 2.9 fusion.121
  204.6 2.7 fusion.122
  207.4 1.3 fusion.123
  208.7 2.5 reshape.1005
  211.2 2.3 gather_fusion.3
  213.5 3.4 %reshape.1009 = f32[128,2,2048]{2,1,0:T(2,128)} reshape(bf16[256,2048]{1,0:T(8,128)(2,1)} %gather_fusion.3) | data formatting | bytes 3145728 | tf_op jit(solution)/shard_map/convert_element_type | solution.py:212
  216.9 4.2 %reduce_sum.44 = f32[128,2048]{1,0:T(8,128)S(1)} reduce(f32[128,2,2048]{2,1,0:T(2,128)} %reshape.1009, f32[]{:T(128)} %constant.138.clone.1), dimensions={1}, to_apply=%region_5.6 | reduce | flops 262144 | bytes 3145732 | tf_op jit(solution)/shard_map/reduce_sum | solution.py:212
  221.4 0.5 copy-done.12
  222.0 6.4 %while.32 = (s32[]{:T(128)}, f32[1,128,256]{2,1,0:T(8,128)S(1)}, bf16[2,1,64,256]{3,2,1,0:T(8,128)(2,1)S(1)}, bf16[2,1,64,128]{3,2,1,0:T(8,128)(2,1)S(1)}, f32[2...) while((s32[]{:T(128)}, f32[1,128,256]{2,1,0:T(8,128)S(1)}, ...), condition=%wide.region_8.9_spmd, body=%wide.region_7.8_spmd.sunk | while | flops 19046464 | bytes 1142157 | solution.py:242
  223.0 0.6 slice.201
  224.3 0.7 subtract_exponential_fusion.4
  226.2 0.6 slice.201
  227.5 0.7 subtract_exponential_fusion.4
  228.4 1.5 convolution_convert_fusion
  229.9 6.9 %all-to-all-start.3 = ((bf16[32,64,256]{2,1,0:T(8,128)(2,1)}), bf16[32,64,256]{2,1,0:T(8,128)(2,1)S(1)}, u32[]{:S(2)}, u32[]{:S(2)}) async-start(bf16[32,64,256]{2,1,0:T(8,128)(2,1)} %bitcast.373), calls=%async_computation.3 | async-start | bytes 2097152 | tf_op jit(solution)/shard_map/all_to_all | solution.py:60
  237.1 13.6 %all-gather = bf16[512,256]{1,0:T(8,128)(2,1)S(1)} all-gather(bf16[128,256]{1,0:T(8,128)(2,1)S(1)} %convolution_convert_fusion.5), channel_id=2, replica_groups=mesh['sp_0'=8,'sp_1'=4,'tp'=16] {'sp_1'}, dimensions={0}, use_global_device_ids=true | all-gather | bytes 327680 | tf_op jit(solution)/shard_map/all_gather | solution.py:37
  250.7 1.9 fusion.138
  252.6 26.5 %all_gather.31 = bf16[8,1,128,256]{3,2,1,0:T(8,128)(2,1)S(1)} all-gather(bf16[1,1,128,256]{3,2,1,0:T(8,128)(2,1)S(1)} %fusion.138), channel_id=1, replica_groups=mesh['sp_0'=8,'sp_1'=4,'tp'=16] {'sp_0'}, dimensions={0}, use_global_device_ids=true | all-gather | bytes 589824 | tf_op jit(solution)/shard_map/all_gather | solution.py:37
  279.1 2.1 fusion.137
  281.2 6.6 %while.33 = (s32[]{:T(128)}, f32[1,128,256]{2,1,0:T(8,128)S(1)}, f32[2,1,64,128]{3,2,1,0:T(8,128)S(1)}, bf16[2,1,64,256]{3,2,1,0:T(8,128)(2,1)S(1)}, f32[2,1,64]...) while((s32[]{:T(128)}, f32[1,128,256]{2,1,0:T(8,128)S(1)}, ...), condition=%wide.region_12.13_spmd, body=%wide.region_11.12_spmd.sunk | while | flops 19046468 | bytes 1142169 | solution.py:251
  281.3 0.6 slice.202
  281.8 0.7 subtract_exponential_fusion.5
  284.6 0.6 slice.202
  285.2 0.7 subtract_exponential_fusion.5
  287.9 0.6 multiply_convert_fusion.4
  288.5 0.8 convert_reduce_fusion
  (114 shorter events, 9.0 us)
Async XLA Ops:
  7.2 213.9 %copy-start = (bf16[2048,256]{1,0:T(8,128)(2,1)S(1)}, bf16[2048,256]{1,0:T(8,128)(2,1)}, u32[]{:S(2)}) copy-start(bf16[2048,256]{1,0:T(8,128)(2,1)} %param.24) | copy-start | bytes 3145732
  7.2 4.7 %copy-start.1 = (bf16[128,2048]{1,0:T(8,128)(2,1)S(1)}, bf16[128,2048]{1,0:T(8,128)(2,1)}, u32[]{:S(2)}) copy-start(bf16[128,2048]{1,0:T(8,128)(2,1)} %param.18) | copy-start | bytes 1572868
  7.2 85.5 %all-gather.5.cloned.1.call-start = ((), (), s32[]{:S(2)}) async-start(), calls=%async_computation.4 | async-start | bytes 2785280 | tf_op jit(solution)/shard_map/all_gather | solution.py:21
  14.4 2.1 copy-start.15
  16.5 2.9 copy-start.2
  24.4 68.3 %copy-start.6 = (bf16[1,2048,128]{2,1,0:T(8,128)(2,1)S(1)}, bf16[1,2048,128]{2,1,0:T(8,128)(2,1)}, u32[]{:S(2)}) copy-start(bf16[1,2048,128]{2,1,0:T(8,128)(2,1)} %param.21) | copy-start | bytes 1572868
  50.8 43.9 %copy-start.7 = (bf16[1,2048,128]{2,1,0:T(8,128)(2,1)S(1)}, bf16[1,2048,128]{2,1,0:T(8,128)(2,1)}, u32[]{:S(2)}) copy-start(bf16[1,2048,128]{2,1,0:T(8,128)(2,1)} %param.22) | copy-start | bytes 1572868
  50.8 157.8 %all-gather.7.cloned.1.call-start = ((), (), s32[]{:S(2)}) async-start(), calls=%async_computation.5 | async-start | bytes 2228224 | tf_op jit(solution)/shard_map/all_gather | solution.py:207
  92.7 3.9 %copy-start.4 = (bf16[2,320,2048]{2,1,0:T(8,128)(2,1)S(1)}, bf16[2,320,2048]{2,1,0:T(8,128)(2,1)}, u32[]{:S(2)}) copy-start(bf16[2,320,2048]{2,1,0:T(8,128)(2,1)} %all-gather.5.cloned.1.call-done) | copy-start | bytes 7864324
  94.7 1.9 copy-start.16
  97.1 0.6 copy-start.9
  137.3 22.6 %copy-start.17 = (f32[1,128]{1,0:T(1,128)S(1)}, f32[1,128]{1,0:T(1,128)}, u32[]{:S(2)}) copy-start(f32[1,128]{1,0:T(1,128)} %param.28) | copy-start | bytes 1540
  137.3 54.3 %copy-start.8 = (bf16[1,128,128]{2,1,0:T(8,128)(2,1)S(1)}, bf16[1,128,128]{2,1,0:T(8,128)(2,1)}, u32[]{:S(2)}) copy-start(bf16[1,128,128]{2,1,0:T(8,128)(2,1)} %param.25) | copy-start | bytes 98308
  137.5 64.2 %copy-start.13 = (bf16[1,128,128]{2,1,0:T(8,128)(2,1)S(1)}, bf16[1,128,128]{2,1,0:T(8,128)(2,1)}, u32[]{:S(2)}) copy-start(bf16[1,128,128]{2,1,0:T(8,128)(2,1)} %param.26) | copy-start | bytes 98308
  159.9 44.8 %copy-start.10 = (bf16[320,128]{1,0:T(8,128)(2,1)S(1)}, bf16[320,128]{1,0:T(8,128)(2,1)}, u32[]{:S(2)}) copy-start(bf16[320,128]{1,0:T(8,128)(2,1)} %copy-done.9) | copy-start | bytes 245764
  201.7 5.7 %copy-start.5 = (bf16[2,320,2048]{2,1,0:T(8,128)(2,1)S(1)}, bf16[2,320,2048]{2,1,0:T(8,128)(2,1)}, u32[]{:S(2)}) copy-start(bf16[2,320,2048]{2,1,0:T(8,128)(2,1)} %all-gather.5.cloned.1.call-done) | copy-start | bytes 7864324
  221.1 0.8 copy-start.12
  221.1 0.9 copy-start.3
  228.4 1.5 copy-start.14
  229.9 58.6 %all-to-all-start.3 = ((bf16[32,64,256]{2,1,0:T(8,128)(2,1)}), bf16[32,64,256]{2,1,0:T(8,128)(2,1)S(1)}, u32[]{:S(2)}, u32[]{:S(2)}) async-start(bf16[32,64,256]{2,1,0:T(8,128)(2,1)} %bitcast.373), calls=%async_computation.3 | async-start | bytes 2097152 | tf_op jit(solution)/shard_map/all_to_all | solution.py:60
  287.9 1.4 copy-start.11
Sparse Core Ops, SparseCore 0:
  50.9 41.6 all-gather.4
  160.0 35.0 all-gather.6
where the time goes:
time: 297 us; the launch traced here: 296 us
  blocking collectives  146 us (49%)
  waiting for transfers between devices  41.8 us (14%)
  local copies, waits for them, and re-layouts  34.9 us (12%)
  between operations  23.5 us (8%)
  other arithmetic  20.7 us (7%)
  matrix products  19.4 us (7%)
  starting transfers between devices  6.99 us (2%)
  loops' own time  3 us (1%)
    all_gather x1, waiting for transfers between devices, in_one_piece(): whole = lax.all_gather(both, axis, axis=dim, tiled=True)  41.8 us
    all_gather x2, blocking collectives, prefix_by_axis(): lax.all_gather(part.astype(kind), axis)  40.1 us
    all_to_all x1, blocking collectives, body(): lax.all_to_all(grouped, 'tp', split_axis=2, concat_axis=2, tiled=True)  38.4 us
    all_to_all x1, blocking collectives, sent_together(): lax.all_to_all(both, axis, split_axis=split_dim, concat_axis=concat_dim,...  24.4 us
    unnamed x2, blocking collectives  23.5 us
    all_to_all x1, blocking collectives, body(): lax.all_to_all(feature_part, SP, split_axis=1, concat_axis=0, tiled=True)  19.3 us
    unnamed x49, local copies, waits for them, and re-layouts  7.78 us
    all_to_all x1, starting transfers between devices, summed_on_arrival(): lax.all_to_all(pieces, axis, split_axis=0, concat_axis=0, tiled=True)  6.91 us
  transfers between devices with their start and end apart: 3, of which 1 were waited for; matrix products, arithmetic and copies ran while one was open for 9% of the time, Pallas kernels for 0%

commit v1 on v0

--- a/solution.py
+++ b/solution.py
@@ -1,25 +1,418 @@
+import functools
+
 import jax
 import jax.numpy as jnp
 from jax import lax
+from jax.experimental import pallas as pl
+from jax.experimental.pallas import tpu as pltpu
 from jax.sharding import Mesh
 from jax.sharding import PartitionSpec as P
 
 BLOCK = 64
 SP = ("sp_0", "sp_1")
-
-
-def sent_together(arrays, axis, split_dim, concat_dim, along):
-    widths = [a.shape[along] for a in arrays]
-    both = jnp.concatenate(arrays, axis=along)
-    whole = lax.all_to_all(both, axis, split_axis=split_dim, concat_axis=concat_dim, tiled=True)
-    return tuple(jnp.split(whole, [sum(widths[:k]) for k in range(1, len(widths))], axis=along))
-
-
-def in_one_piece(arrays, axis, dim, along):
-    widths = [a.shape[along] for a in arrays]
-    both = jnp.concatenate(arrays, axis=along)
-    whole = lax.all_gather(both, axis, axis=dim, tiled=True)
-    return tuple(jnp.split(whole, [sum(widths[:k]) for k in range(1, len(widths))], axis=along))
+BF = jnp.bfloat16
+F32 = jnp.float32
+MSG = 16
+
+
+def mm(a, b, dims=((1,), (0,))):
+    return lax.dot_general(a, b, (dims, ((), ())), preferred_element_type=F32)
+
+
+def silu_slope_of(v, sig):
+    return sig * (1.0 + v * (1.0 - sig))
+
+
+def front_kernel(
+    sizes,
+    x_hbm, g_hbm, routes_ref, rw_ref, wg_hbm, wu_hbm, wd_hbm,
+    gg_ref, ug_ref, dg_ref, mix_ref,
+    xs, gs, wgu, wd, pt, send, recv, rows, acc_gu, acc_hb, gbub, hid,
+    part, part_in, out_r, out_l, in_r, in_l, back, ret, mixed,
+    load_sem, a2a_send, a2a_recv, ag_send, ag_recv, pp_send, pp_recv,
+    rs_send, rs_recv, ret_send, ret_recv, mg_send, mg_recv,
+):
+    n_sp, n_tp, cap, slots = sizes
+    n_chip = n_tp // 2
+    half = n_chip // 2
+    tok = x_hbm.shape[0]
+    width = xs.shape[1]
+    n_rows = n_sp * cap
+    hr = n_rows // 2
+    s, t = lax.axis_index("sp"), lax.axis_index("tp")
+    chip, par = t // 2, t % 2
+    partner = t + 1 - 2 * par
+
+    def tp_of(c, parity=None):
+        return lax.rem(c + 2 * n_chip, n_chip) * 2 + (par if parity is None else parity)
+
+    right, left = tp_of(chip + 1), tp_of(chip - 1)
+
+    def remote(src, dst, ssem, rsem, where):
+        return pltpu.make_async_remote_copy(
+            src_ref=src, dst_ref=dst, send_sem=ssem, recv_sem=rsem,
+            device_id=where, device_id_type=pl.DeviceIdType.MESH,
+        )
+
+    share = pl.ds(pl.multiple_of(t * width, width), width)
+    loads = [
+        pltpu.make_async_copy(x_hbm.at[:, share], xs, load_sem.at[0]),
+        pltpu.make_async_copy(g_hbm.at[:, share], gs, load_sem.at[1]),
+        pltpu.make_async_copy(wg_hbm, wgu.at[:, pl.ds(0, width)], load_sem.at[2]),
+        pltpu.make_async_copy(wu_hbm, wgu.at[:, pl.ds(width, width)], load_sem.at[3]),
+        pltpu.make_async_copy(wd_hbm, wd, load_sem.at[4]),
+    ]
+    for c in loads:
+        c.start()
+
+    recv[...] = jnp.zeros_like(recv)
+    ret[...] = jnp.zeros_like(ret)
+    barrier = pltpu.get_barrier_semaphore()
+
+    def greet_sp(d, carry):
+        pl.semaphore_signal(
+            barrier, inc=1, device_id={"sp": lax.rem(s + d, n_sp), "tp": t},
+            device_id_type=pl.DeviceIdType.MESH)
+        return carry
+
+    def greet_tp(d, carry):
+        pl.semaphore_signal(
+            barrier, inc=1, device_id={"sp": s, "tp": tp_of(chip + d)},
+            device_id_type=pl.DeviceIdType.MESH)
+        return carry
+
+    lax.fori_loop(1, n_sp, greet_sp, 0)
+    lax.fori_loop(1, n_chip, greet_tp, 0)
+    pl.semaphore_signal(barrier, inc=1, device_id={"sp": s, "tp": partner},
+                        device_id_type=pl.DeviceIdType.MESH)
+
+    r0, r1 = routes_ref[:, 0:1], routes_ref[:, 1:2]
+    lane = lax.broadcasted_iota(jnp.int32, (tok, n_sp * slots), 1)
+    expert, place = lane // slots, lane % slots
+    first, second = r0 == expert, r1 == expert
+    named = jnp.where(first | second, 1.0, 0.0)
+    row_i = lax.broadcasted_iota(jnp.int32, (tok, tok), 0)
+    col_i = lax.broadcasted_iota(jnp.int32, (tok, tok), 1)
+    earlier = jnp.where(col_i < row_i, 1.0, 0.0).astype(BF)
+    count = mm(earlier, named.astype(BF))
+    here = count == place.astype(F32)
+    p0 = jnp.where(first & here, 1.0, 0.0).astype(BF)
+    p1 = jnp.where(second & here, 1.0, 0.0).astype(BF)
+    pt[...] = jnp.where((first | second) & here, 1.0, 0.0).astype(BF)
+    loads[0].wait()
+    loads[1].wait()
+    gf = gs[...].astype(F32)
+    sg0 = (rw_ref[:, 0:1] * gf).astype(BF)
+    sg1 = (rw_ref[:, 1:2] * gf).astype(BF)
+    xv = xs[...]
+    sendrows = mm(p0, jnp.concatenate([xv, sg0], axis=1), ((0,), (0,)))
+    sendrows += mm(p1, jnp.concatenate([xv, sg1], axis=1), ((0,), (0,)))
+    send[...] = sendrows.astype(BF)
+
+    pl.semaphore_wait(barrier, n_sp - 1 + n_chip - 1 + 1)
+
+    def block(ref, e, length=slots):
+        return ref.at[pl.ds(pl.multiple_of(e * slots, slots), length)]
+
+    def dispatch(d, carry):
+        e = lax.rem(s + d, n_sp)
+        remote(block(send, e, MSG), block(recv, s, MSG), a2a_send.at[e], a2a_recv.at[s],
+               {"sp": e, "tp": t}).start()
+        return carry
+
+    lax.fori_loop(1, n_sp, dispatch, 0)
+    recv[pl.ds(pl.multiple_of(s * slots, slots), slots), :] = send[
+        pl.ds(pl.multiple_of(s * slots, slots), slots), :]
+
+    def arrived(d, carry):
+        e = lax.rem(s + d, n_sp)
+        c = remote(block(send, e, MSG), block(recv, e, MSG), a2a_send.at[e], a2a_recv.at[e],
+                   {"sp": e, "tp": t})
+        c.wait()
+        return carry
+
+    lax.fori_loop(1, n_sp, arrived, 0)
+
+    dense_r = lax.broadcasted_iota(jnp.int32, (n_rows, n_sp * slots), 0)
+    padded_c = lax.broadcasted_iota(jnp.int32, (n_rows, n_sp * slots), 1)
+    squeeze = jnp.where(
+        padded_c == (dense_r // cap) * slots + dense_r % cap, 1.0, 0.0).astype(BF)
+    packed = mm(squeeze, recv[...]).astype(BF)
+    rows[t, 0] = packed[:, :width]
+    rows[t, 1] = packed[:, width:]
+
+    started = []
+
+    def pass_on(origin, u, where, k):
+        c = remote(rows.at[origin, u], rows.at[origin, u], ag_send.at[k], ag_recv.at[origin, u],
+                   {"sp": s, "tp": where})
+        c.start()
+        started.append(c)
+
+    def await_rows(origin, u):
+        remote(rows.at[origin, u], rows.at[origin, u], ag_send.at[0], ag_recv.at[origin, u],
+               {"sp": s, "tp": partner}).wait_recv()
+
+    n_sent = 0
+
+    def next_sem():
+        nonlocal n_sent
+        n_sent += 1
+        return n_sent - 1
+
+    def goes(direction, u, k):
+        return k < half or (k == half and u == direction)
+
+    for u in (0, 1):
+        if goes(0, u, 1):
+            pass_on(t, u, right, next_sem())
+        if goes(1, u, 1):
+            pass_on(t, u, left, next_sem())
+    for u in (0, 1):
+        pass_on(t, u, partner, next_sem())
+
+    acc_gu[...] = jnp.zeros_like(acc_gu)
+    acc_hb[...] = jnp.zeros_like(acc_hb)
+    for c in loads[2:]:
+        c.wait()
+
+    def feats(c):
+        return pl.ds(pl.multiple_of(c * 2 * width, 2 * width), 2 * width)
+
+    def forward(c):
+        for u in (0, 1):
+            await_rows(tp_of(c, 1 - par), u)
+        xin = jnp.concatenate([rows[2 * c, 0], rows[2 * c + 1, 0]], axis=1)
+        gin = jnp.concatenate([rows[2 * c, 1], rows[2 * c + 1, 1]], axis=1)
+        acc_gu[...] += mm(xin, wgu[feats(c), :])
+        acc_hb[...] += mm(gin, wd[:, feats(c)], ((1,), (1,)))
+
+    ready = [chip]
+    for k in range(1, half + 1):
+        from_left, from_right = lax.rem(chip - k + n_chip, n_chip), lax.rem(chip + k, n_chip)
+        for u in (0, 1):
+            if goes(0, u, k):
+                o = from_left * 2 + par
+                await_rows(o, u)
+                if goes(0, u, k + 1):
+                    pass_on(o, u, right, next_sem())
+                pass_on(o, u, partner, next_sem())
+            if goes(1, u, k):
+                o = from_right * 2 + par
+                await_rows(o, u)
+                if goes(1, u, k + 1):
+                    pass_on(o, u, left, next_sem())
+                pass_on(o, u, partner, next_sem())
+        for c in ready:
+            forward(c)
+        ready = [from_left, from_right] if k < half else [from_left]
+    for c in ready:
+        forward(c)
+    for c in started:
+        c.wait_send()
+
+    gate_pre, up_pre = acc_gu[:, :width], acc_gu[:, width:]
+    sig = jax.nn.sigmoid(gate_pre)
+    active = gate_pre * sig
+    hb = acc_hb[...]
+    hid[...] = (active * up_pre).astype(BF)
+    gbub[:, :width] = (hb * up_pre * silu_slope_of(gate_pre, sig)).astype(BF)
+    gbub[:, width:] = (hb * active).astype(BF)
+
+    order = [chip + half]
+    for k in range(half - 1, 0, -1):
+        order += [chip + k, chip - k]
+    order = [lax.rem(c + n_chip, n_chip) for c in order + [chip]]
+    shared = []
+    gb_all = gbub[...]
+    for n, c in enumerate(order):
+        value = mm(gb_all, wgu[feats(c), :], ((1,), (1,))).astype(BF)
+        part[c, 0] = value[:, :width]
+        part[c, 1] = value[:, width:]
+        cp = remote(part.at[c, 1 - par], part_in.at[c], pp_send.at[n], pp_recv.at[c],
+                    {"sp": s, "tp": partner})
+        cp.start()
+        shared.append(cp)
+
+    def await_part(c):
+        remote(part.at[c, 1 - par], part_in.at[c], pp_send.at[0], pp_recv.at[c],
+               {"sp": s, "tp": partner}).wait_recv()
+
+    cut = (pl.ds(0, hr), pl.ds(hr, hr))
+    sums = []
+
+    def ring_copy(direction, i, h):
+        out, inn = (out_r, in_r) if direction == 0 else (out_l, in_l)
+        return remote(out.at[i - 1, cut[h]], inn.at[i - 1, cut[h]],
+                      rs_send.at[direction, i - 1, h], rs_recv.at[direction, i - 1, h],
+                      {"sp": s, "tp": right if direction == 0 else left})
+
+    def has(direction, i, h):
+        return i >= 2 or h == direction
+
+    for i in range(1, half + 1):
+        d = half + 1 - i
+        targets = (lax.rem(chip + d, n_chip), lax.rem(chip - d + n_chip, n_chip))
+        if i == 1:
+            await_part(targets[0])
+        else:
+            await_part(targets[0])
+            await_part(targets[1])
+        for h in (0, 1):
+            for direction in (0, 1):
+                if not has(direction, i, h):
+                    continue
+                out, inn = (out_r, in_r) if direction == 0 else (out_l, in_l)
+                c = targets[direction]
+                total = part[c, par, cut[h], :].astype(F32) + part_in[c, cut[h], :].astype(F32)
+                if i >= 2 and has(direction, i - 1, h):
+                    ring_copy(direction, i - 1, h).wait_recv()
+                    total += inn[i - 2, cut[h], :].astype(F32)
+                out[i - 1, cut[h], :] = total.astype(BF)
+                cp = ring_copy(direction, i, h)
+                cp.start()
+                sums.append(cp)
+    await_part(chip)
+    pieces = []
+    for h in (0, 1):
+        total = part[chip, par, cut[h], :].astype(F32) + part_in[chip, cut[h], :].astype(F32)
+        for direction in (0, 1):
+            if has(direction, half, h):
+                ring_copy(direction, half, h).wait_recv()
+                inn = in_r if direction == 0 else in_l
+                total += inn[half - 1, cut[h], :].astype(F32)
+        pieces.append(total.astype(BF))
+    summed = jnp.concatenate(pieces, axis=0)
+
+    padded_r = lax.broadcasted_iota(jnp.int32, (n_sp * slots, n_rows), 0)
+    dense_c = lax.broadcasted_iota(jnp.int32, (n_sp * slots, n_rows), 1)
+    spread = jnp.where(
+        padded_r == (dense_c // cap) * slots + dense_c % cap, 1.0, 0.0).astype(BF)
+    back[...] = mm(spread, summed).astype(BF)
+
+    def send_back(d, carry):
+        e = lax.rem(s + d, n_sp)
+        remote(block(back, e, MSG), block(ret, s, MSG), ret_send.at[e], ret_recv.at[s],
+               {"sp": e, "tp": t}).start()
+        return carry
+
+    lax.fori_loop(1, n_sp, send_back, 0)
+    ret[pl.ds(pl.multiple_of(s * slots, slots), slots), :] = back[
+        pl.ds(pl.multiple_of(s * slots, slots), slots), :]
+
+    hid_all = hid[...]
+    for c in range(n_chip):
+        xin = jnp.concatenate([rows[2 * c, 0], rows[2 * c + 1, 0]], axis=1)
+        gin = jnp.concatenate([rows[2 * c, 1], rows[2 * c + 1, 1]], axis=1)
+        both = mm(xin, gb_all, ((0,), (0,)))
+        at = pl.ds(c * 2 * width, 2 * width)
+        gg_ref[at, :] = both[:, :width].astype(BF)
+        ug_ref[at, :] = both[:, width:].astype(BF)
+        dg_ref[:, at] = mm(hid_all, gin, ((0,), (0,))).astype(BF)
+    for cp in shared + sums:
+        cp.wait_send()
+
+    def returned(d, carry):
+        e = lax.rem(s + d, n_sp)
+        remote(block(back, e, MSG), block(ret, e, MSG), ret_send.at[e], ret_recv.at[e],
+               {"sp": e, "tp": t}).wait()
+        return carry
+
+    lax.fori_loop(1, n_sp, returned, 0)
+    mixed[t] = (gs[...].astype(F32) + mm(pt[...], ret[...])).astype(BF)
+
+    def mixed_copy(origin, where, k):
+        return remote(mixed.at[origin], mixed.at[origin], mg_send.at[k], mg_recv.at[origin],
+                      {"sp": s, "tp": where})
+
+    copies = []
+    for d in range(half, 0, -1):
+        for c in sorted({d, n_chip - d}):
+            cp = mixed_copy(t, tp_of(chip + c), c)
+            cp.start()
+            copies.append(cp)
+    cp = mixed_copy(t, partner, 0)
+    cp.start()
+    copies.append(cp)
+    for d in range(1, half + 1):
+        for c in sorted({d, n_chip - d}):
+            o = tp_of(chip + c)
+            mixed_copy(o, partner, n_chip + c).wait_recv()
+            cp = mixed_copy(o, partner, n_chip + c)
+            cp.start()
+            copies.append(cp)
+    for d in range(n_chip):
+        mixed_copy(tp_of(chip + d, 1 - par), partner, 0).wait_recv()
+    for o in range(n_tp):
+        mix_ref[:, o * width:(o + 1) * width] = mixed[o]
+    for cp in copies:
+        cp.wait_send()
+
+
+def front(n_sp, n_tp, moe_input, out_grad, routes, route_weight, w_gate, w_up, w_down):
+    tok, model = moe_input.shape
+    cap = 5 * tok * routes.shape[1] // (4 * n_sp)
+    slots = -(-cap // 16) * 16
+    width = model // n_tp
+    hidden = w_gate.shape[1]
+    n_rows = n_sp * cap
+    n_chip = n_tp // 2
+    half = n_chip // 2
+    hbm = pl.BlockSpec(memory_space=pl.ANY)
+    vmem = pl.BlockSpec(memory_space=pltpu.VMEM)
+    dma = pltpu.SemaphoreType.DMA
+    n_ag = 2 * (2 * half - 1) + 2 * n_chip
+    return pl.pallas_call(
+        functools.partial(front_kernel, (n_sp, n_tp, cap, slots)),
+        name="front",
+        out_shape=(
+            jax.ShapeDtypeStruct((model, hidden), BF),
+            jax.ShapeDtypeStruct((model, hidden), BF),
+            jax.ShapeDtypeStruct((hidden, model), BF),
+            jax.ShapeDtypeStruct((tok, model), BF),
+        ),
+        in_specs=[hbm, hbm, vmem, vmem, hbm, hbm, hbm],
+        out_specs=(vmem, vmem, vmem, vmem),
+        scratch_shapes=[
+            pltpu.VMEM((tok, width), BF),
+            pltpu.VMEM((tok, width), BF),
+            pltpu.VMEM((model, 2 * hidden), BF),
+            pltpu.VMEM((hidden, model), BF),
+            pltpu.VMEM((tok, n_sp * slots), BF),
+            pltpu.VMEM((n_sp * slots, 2 * width), BF),
+            pltpu.VMEM((n_sp * slots, 2 * width), BF),
+            pltpu.VMEM((n_tp, 2, n_rows, width), BF),
+            pltpu.VMEM((n_rows, 2 * hidden), F32),
+            pltpu.VMEM((n_rows, hidden), F32),
+            pltpu.VMEM((n_rows, 2 * hidden), BF),
+            pltpu.VMEM((n_rows, hidden), BF),
+            pltpu.VMEM((n_chip, 2, n_rows, width), BF),
+            pltpu.VMEM((n_chip, n_rows, width), BF),
+            pltpu.VMEM((half, n_rows, width), BF),
+            pltpu.VMEM((half, n_rows, width), BF),
+            pltpu.VMEM((half, n_rows, width), BF),
+            pltpu.VMEM((half, n_rows, width), BF),
+            pltpu.VMEM((n_sp * slots, width), BF),
+            pltpu.VMEM((n_sp * slots, width), BF),
+            pltpu.VMEM((n_tp, tok, width), BF),
+            dma((5,)),
+            dma((n_sp,)),
+            dma((n_sp,)),
+            dma((n_ag,)),
+            dma((n_tp, 2)),
+            dma((n_chip,)),
+            dma((n_chip,)),
+            dma((2, half, 2)),
+            dma((2, half, 2)),
+            dma((n_sp,)),
+            dma((n_sp,)),
+            dma((2 * n_chip,)),
+            dma((n_tp,)),
+        ],
+        compiler_params=pltpu.CompilerParams(
+            collective_id=0, has_side_effects=True, vmem_limit_bytes=48 << 20
+        ),
+    )(moe_input, out_grad, routes, route_weight, w_gate, w_up, w_down)
 
 
 def neutral_like(shard, identity):
@@ -123,94 +516,8 @@
     )
 
 
-def expert_backward(rows_in, grad_in, w_gate, w_up, w_down):
-    gate_pre = jnp.einsum("erd,edf->erf", rows_in, w_gate, preferred_element_type=jnp.float32)
-    up_pre = jnp.einsum("erd,edf->erf", rows_in, w_up, preferred_element_type=jnp.float32)
-    active = jax.nn.silu(gate_pre)
-    hidden = (active * up_pre).astype(jnp.bfloat16)
-    hidden_back = jnp.einsum("erd,efd->erf", grad_in, w_down, preferred_element_type=jnp.float32)
-    down_part = jnp.einsum("erf,erd->efd", hidden, grad_in, preferred_element_type=jnp.float32)
-    gate_back = (hidden_back * up_pre * silu_slope(gate_pre)).astype(jnp.bfloat16)
-    up_back = (hidden_back * active).astype(jnp.bfloat16)
-    gate_part = jnp.einsum("erd,erf->edf", rows_in, gate_back, preferred_element_type=jnp.float32)
-    up_part = jnp.einsum("erd,erf->edf", rows_in, up_back, preferred_element_type=jnp.float32)
-    partial_value = jnp.einsum(
-        "erf,edf->erd", gate_back, w_gate, preferred_element_type=jnp.float32
-    )
-    partial_value = partial_value + jnp.einsum(
-        "erf,edf->erd", up_back, w_up, preferred_element_type=jnp.float32
-    )
-    return (
-        gate_part.astype(jnp.bfloat16),
-        up_part.astype(jnp.bfloat16),
-        down_part.astype(jnp.bfloat16),
-        partial_value.astype(jnp.bfloat16),
-    )
-
-
-def body(
-    moe_input,
-    out_grad,
-    routes,
-    route_weight,
-    w_gate,
-    w_up,
-    w_down,
-    w_out,
-    query_heads,
-    key_heads,
-    value_heads,
-    log_decay,
-    state_in,
-):
-    tok_rows, model_width = moe_input.shape
-    picks = routes.shape[1]
-    experts = w_gate.shape[0] * lax.axis_size(SP)
-    capacity = 5 * tok_rows * picks // (4 * experts)
-    route_ids = routes.reshape(-1)
-    routed = route_ids.shape[0]
-    onehot = (route_ids[:, None] == jnp.arange(experts, dtype=jnp.int32)[None, :]).astype(jnp.int32)
-    slot_index = jnp.sum(jnp.cumsum(onehot, axis=0) * onehot, axis=1) - 1
-    target = route_ids * capacity + slot_index
-    source = (
-        jnp.full((experts * capacity,), routed, jnp.int32)
-        .at[target]
-        .set(jnp.arange(routed, dtype=jnp.int32))
-    )
-    filled = source < routed
-    picked = jnp.where(filled, source, 0)
-    token_idx = picked // picks
-    weight_slot = jnp.where(filled, route_weight.reshape(-1)[picked], 0.0)
-    send_rows = jnp.where(filled[:, None], moe_input[token_idx], jnp.zeros((), jnp.bfloat16))
-    send_rows = send_rows.reshape(experts, capacity, model_width)
-    send_grad = (weight_slot[:, None] * out_grad[token_idx].astype(jnp.float32)).astype(
-        jnp.bfloat16
-    )
-    send_grad = send_grad.reshape(experts, capacity, model_width)
-    group_count = lax.axis_size("tp")
-    slice_width = model_width // group_count
-    offset = lax.axis_index("tp") * slice_width
-    pieces = (
-        lax.dynamic_slice_in_dim(send_rows, offset, slice_width, 2),
-        lax.dynamic_slice_in_dim(send_grad, offset, slice_width, 2),
-    )
-    pieces = sent_together((pieces[0], pieces[1]), SP, 0, 1, 2)
-    rows_in, grad_in = in_one_piece((pieces[0], pieces[1]), "tp", 2, 0)
-    gate_grad, up_grad, down_grad, partial_value = expert_backward(
-        rows_in, grad_in, w_gate, w_up, w_down
-    )
-    local_rows = partial_value.shape[1]
-    grouped = partial_value.reshape(partial_value.shape[0], local_rows, group_count, slice_width)
-    spread_parts = lax.all_to_all(grouped, "tp", split_axis=2, concat_axis=2, tiled=True)
-    feature_part = jnp.sum(spread_parts.astype(jnp.float32), axis=2).astype(jnp.bfloat16)
-    returned_part = lax.all_to_all(feature_part, SP, split_axis=1, concat_axis=0, tiled=True)
-    returned = lax.all_gather(returned_part, "tp", axis=2, tiled=True)
-    gathered = returned.reshape(experts * capacity, model_width)[target].reshape(
-        tok_rows, picks, model_width
-    )
-    mixed_grad = (
-        out_grad.astype(jnp.float32) + jnp.sum(gathered.astype(jnp.float32), axis=1)
-    ).astype(jnp.bfloat16)
+def tail(mixed_grad, w_out, query_heads, key_heads, value_heads, log_decay, state_in):
+    tok_rows = mixed_grad.shape[0]
     head_count = query_heads.shape[0]
     key_size = key_heads.shape[-1]
     value_size = value_heads.shape[-1]
@@ -265,22 +572,39 @@
     query_gradient = from_blocks(query_gradient).astype(jnp.bfloat16)
     key_grad = (from_blocks(key_grad) * key_size ** (-0.5)).astype(jnp.bfloat16)
     value_grad = from_blocks(value_grad).astype(jnp.bfloat16)
-    return (gate_grad, up_grad, down_grad, out_proj_grad, query_gradient, key_grad, value_grad)
+    return (out_proj_grad, query_gradient, key_grad, value_grad)
 
 
 def solution(mesh):
-    finer = Mesh(mesh.devices.reshape(8, 4, mesh.shape["tp"]), ("sp_0", "sp_1", "tp"))
-    return jax.shard_map(
-        body,
+    n_sp, n_tp = mesh.shape["sp"], mesh.shape["tp"]
+    finer = Mesh(mesh.devices.reshape(8, 4, n_tp), ("sp_0", "sp_1", "tp"))
+
+    def first(moe_input, out_grad, routes, route_weight, w_gate, w_up, w_down):
+        gate_grad, up_grad, down_grad, mixed = front(
+            n_sp, n_tp, moe_input, out_grad, routes, route_weight, w_gate[0], w_up[0], w_down[0]
+        )
+        return gate_grad[None], up_grad[None], down_grad[None], mixed
+
+    first = jax.shard_map(
+        first,
+        mesh=mesh,
+        in_specs=(
+            P("sp", None),
+            P("sp", None),
+            P("sp", None),
+            P("sp", None),
+            P("sp", None, "tp"),
+            P("sp", None, "tp"),
+            P("sp", "tp", None),
+        ),
+        out_specs=(P("sp", None, "tp"), P("sp", None, "tp"), P("sp", "tp", None), P("sp", None)),
+        check_vma=False,
+    )
+    second = jax.shard_map(
+        tail,
         mesh=finer,
         in_specs=(
             P(SP, None),
-            P(SP, None),
-            P(SP, None),
-            P(SP, None),
-            P(SP, None, "tp"),
-            P(SP, None, "tp"),
-            P(SP, "tp", None),
             P(None, "tp"),
             P("tp", SP, None),
             P("tp", SP, None),
@@ -288,14 +612,16 @@
             P("tp", SP),
             P("tp", SP, None, None),
         ),
-        out_specs=(
-            P(SP, None, "tp"),
-            P(SP, None, "tp"),
-            P(SP, "tp", None),
-            P(SP, "tp"),
-            P("tp", SP, None),
-            P("tp", SP, None),
-            P("tp", SP, None),
-        ),
+        out_specs=(P(SP, "tp"), P("tp", SP, None), P("tp", SP, None), P("tp", SP, None)),
         check_vma=False,
     )
+
+    def whole(
+        moe_input, out_grad, routes, route_weight, w_gate, w_up, w_down, w_out,
+        query_heads, key_heads, value_heads, log_decay, state_in,
+    ):
+        *grads, mixed = first(moe_input, out_grad, routes, route_weight, w_gate, w_up, w_down)
+        rest = second(mixed, w_out, query_heads, key_heads, value_heads, log_decay, state_in)
+        return (*grads, *rest)
+
+    return whole

time: 297 us -> 225 us (0.76)
  the two profiles are of different devices: /device:TPU:6 before, /device:TPU:8 now
where the time goes in v1:
time: 225 us; the launch traced here: 224 us
  Pallas kernels  77.5 us (34%)
  blocking collectives  71.7 us (32%)
  local copies, waits for them, and re-layouts  21.7 us (10%)
  other arithmetic  17.6 us (8%)
  matrix products  16.8 us (7%)
  between operations  9.43 us (4%)
  starting transfers between devices  5.78 us (3%)
  loops' own time  3.07 us (1%)
    pallas_call x1, Pallas kernels, front(): pl.pallas_call(functools.partial(front_kernel, (n_sp, n_tp, cap, slots)),...  77.5 us
    all_gather x2, blocking collectives, prefix_by_axis(): lax.all_gather(part.astype(kind), axis)  43.8 us
    unnamed x2, blocking collectives  27.9 us
    unnamed x38, local copies, waits for them, and re-layouts  14.9 us
    all_to_all x1, starting transfers between devices, summed_on_arrival(): lax.all_to_all(pieces, axis, split_axis=0, concat_axis=0, tiled=True)  5.78 us
  transfers between devices with their start and end apart: 1, of which 0 were waited for; matrix products, arithmetic and copies ran while one was open for 7% of the time, Pallas kernels for 0%

profile of v1, /device:TPU:8, one launch (start us, length us, event | category | flops | bytes accessed | tf_op | source)
XLA Modules:
  0.0 223.5 jit_solution(12987050665468386554)
XLA Ops:
  0.7 0.6 broadcast_convert_fusion
  1.3 1.0 reduce_window_sum.26
  2.2 0.6 slice.90
  3.5 0.8 copy.33.routes_ref
  4.3 0.8 copy.34.rw_ref
  5.1 0.8 convert_multiply_fusion
  5.8 0.8 convert.34
  6.6 0.5 broadcast.469
  7.1 1.3 reduce.3
  8.5 1.0 copy-done.1
  9.6 1.0 copy-done.2
  10.6 1.0 copy-done.3
  11.7 1.0 copy-done.4
  12.7 1.0 copy-done.5
  13.7 77.5 %front.1 = (bf16[2048,128]{1,0:T(8,128)(2,1)S(1)}, bf16[2048,128]{1,0:T(8,128)(2,1)S(1)}, bf16[128,2048]{1,0:T(8,128)(2,1)S(1)}, bf16[128,2048]{1,0:T(8,128)(2,1)S(1)}) custom-call(bf16[128,2048]{1,0:T(8,128)(2,1)S(1)} %copy-done.1, bf16[128,2048]{1,0:T(8,128)(2,1)S(1)} %copy-done.2, s32[128,2]{1,0:T(8,128)S(1)} %copy.33.routes_ref, ...), custom_call_target="tpu_custom_call" | custom-call | tf_op jit(solution)/shard_map/front/pallas_call | solution.py:365
  91.6 0.5 copy-done.12
  92.1 0.8 fusion.138
  92.9 0.5 reduce_window_sum.25
  93.3 0.6 broadcast.383.clone
  94.0 15.5 %while.32 = (s32[]{:T(128)}, f32[1,128,256]{2,1,0:T(8,128)S(1)}, bf16[2,1,64,256]{3,2,1,0:T(8,128)(2,1)}, bf16[2,1,64,128]{3,2,1,0:T(8,128)(2,1)}, f32[2,1,64]{2...) while((s32[]{:T(128)}, f32[1,128,256]{2,1,0:T(8,128)S(1)}, ...), condition=%wide.region_2.4_spmd, body=%wide.region_1.3_spmd.sunk | while | flops 19046464 | bytes 1142401 | solution.py:549
  94.0 1.0 fusion.215
  95.0 0.8 fusion.216
  95.8 1.1 fusion.217
  96.9 1.6 fusion.218
  98.6 0.7 slice.183
  99.2 0.7 subtract_exponential_fusion.4
  100.7 1.1 fusion.214
  101.8 1.0 fusion.215
  102.8 0.8 fusion.216
  103.6 1.1 fusion.217
  104.7 1.6 fusion.218
  106.4 0.7 slice.183
  107.0 0.7 subtract_exponential_fusion.4
  108.5 1.1 fusion.214
  109.5 2.3 %fusion.120 = bf16[2048,256]{0,1:T(8,128)(2,1)} fusion(bf16[128,256]{1,0:T(8,128)(2,1)} %bitcast.326, bf16[128,2048]{1,0:T(8,128)(2,1)S(1)} %get-tuple-element.235), kind=kOutput, calls=%fused_computation.119 | convolution fusion | flops 134742016 | bytes 1638400 | tf_op jit(solution)/shard_map/dot_general | solution.py:566
  111.9 2.3 %copy.37 = bf16[2048,256]{1,0:T(8,128)(2,1)} copy(bf16[2048,256]{0,1:T(8,128)(2,1)} %fusion.120) | data formatting | bytes 2097152 | tf_op jit(solution)/shard_map/convert_element_type | solution.py:568
  114.1 1.3 dynamic-slice
  115.4 0.8 dynamic-update-slice
  116.1 5.8 %all-to-all-start = ((bf16[32,64,256]{2,1,0:T(8,128)(2,1)}), bf16[32,64,256]{2,1,0:T(8,128)(2,1)}, u32[]{:S(2)}, u32[]{:S(2)}) async-start(bf16[32,64,256]{2,1,0:T(8,128)(2,1)} %bitcast.324), calls=%async_computation | async-start | bytes 2097152 | tf_op jit(solution)/shard_map/all_to_all | solution.py:453
  121.9 10.7 %all-reduce = bf16[4]{0:T(256)(128)(2,1)S(1)} all-reduce(bf16[4]{0:T(256)(128)(2,1)S(1)} %dynamic-update-slice), channel_id=1, replica_groups=mesh['sp_0'=8,'sp_1'=4,'tp'=16] {'sp_1'}, use_global_device_ids=true, to_apply=%add | all-reduce | flops 4 | bytes 16
  132.6 0.6 slice_convert_fusion
  133.2 0.6 fusion.141
  134.1 13.7 %all-gather = bf16[512,256]{1,0:T(8,128)(2,1)S(1)} all-gather(bf16[128,256]{1,0:T(8,128)(2,1)S(1)} %convolution_convert_fusion.2), channel_id=2, replica_groups=mesh['sp_0'=8,'sp_1'=4,'tp'=16] {'sp_1'}, dimensions={0}, use_global_device_ids=true | all-gather | bytes 327680 | tf_op jit(solution)/shard_map/all_gather | solution.py:430
  148.5 2.1 fusion.123
  150.6 30.1 %all_gather.23 = bf16[8,1,128,256]{3,2,1,0:T(8,128)(2,1)} all-gather(bf16[1,1,128,256]{3,2,1,0:T(8,128)(2,1)S(1)} %fusion.123), channel_id=1, replica_groups=mesh['sp_0'=8,'sp_1'=4,'tp'=16] {'sp_0'}, dimensions={0}, use_global_device_ids=true | all-gather | bytes 589824 | tf_op jit(solution)/shard_map/all_gather | solution.py:430
  180.7 1.3 dynamic-slice.1
  182.0 1.4 dynamic-update-slice.1
  183.4 17.2 %all-reduce.1 = bf16[8]{0:T(256)(128)(2,1)S(1)} all-reduce(bf16[8]{0:T(256)(128)(2,1)S(1)} %dynamic-update-slice.1), channel_id=3, replica_groups=mesh['sp_0'=8,'sp_1'=4,'tp'=16] {'sp_0'}, use_global_device_ids=true, to_apply=%add.1 | all-reduce | flops 8 | bytes 32
  200.6 0.7 fusion.140
  208.6 3.3 %fusion.122 = f32[1,128,256]{2,1,0:T(8,128)S(1)} fusion(bf16[8,1,128,256]{3,2,1,0:T(8,128)(2,1)} %all_gather.23, f32[]{:T(128)} %bitcast.52, f32[]{:T(128)S(6)} %convert.22, f32[]{:T(128)} %bitcast.53, f32[]{:T(128)S(6)} %convert.23, f32[]{:T(128)} %bitcast.54, f32[]{:T(128)S(6)} %convert.24, f32[]{:T(128)} %bitcast.55, f32[]{:T(128)S(6)} %convert.25, ...), kind=kLoop, calls=%fused_computation.126 | loop fusion | flops 1572864 | bytes 917568 | tf_op jit(solution)/shard_map/add | solution.py:515
  211.9 6.6 %while.33 = (s32[]{:T(128)}, f32[1,128,256]{2,1,0:T(8,128)S(1)}, f32[2,1,64,128]{3,2,1,0:T(8,128)S(1)}, bf16[2,1,64,256]{3,2,1,0:T(8,128)(2,1)S(1)}, f32[2,1,64]...) while((s32[]{:T(128)}, f32[1,128,256]{2,1,0:T(8,128)S(1)}, ...), condition=%wide.region_6.8_spmd, body=%wide.region_5.7_spmd.sunk | while | flops 19046468 | bytes 1142161 | solution.py:558
  211.9 0.6 slice.184
  212.5 0.7 subtract_exponential_fusion.5
  213.1 0.3 fusion.235
  213.7 0.3 fusion.233
  215.2 0.6 slice.184
  215.8 0.7 subtract_exponential_fusion.5
  216.5 0.3 fusion.235
  217.0 0.3 fusion.233
  218.5 0.6 multiply_convert_fusion
  219.2 2.0 convert_reduce_fusion
  221.2 0.8 copy.77
  222.0 0.8 copy.78
  222.8 0.8 copy.79
  (43 shorter events, 2.1 us)
Async XLA Ops:
  0.6 90.6 %copy-start = (bf16[2048,256]{1,0:T(8,128)(2,1)S(1)}, bf16[2048,256]{1,0:T(8,128)(2,1)}, u32[]{:S(2)}) copy-start(bf16[2048,256]{1,0:T(8,128)(2,1)} %param.25) | copy-start | bytes 3145732
  8.5 1.0 copy-start.1
  9.6 1.0 copy-start.2
  10.6 1.0 copy-start.3
  11.6 1.0 copy-start.4
  12.7 1.0 copy-start.5
  91.2 0.8 copy-start.12
  91.3 2.7 %copy-start.6 = (f32[1,1,128,256]{3,2,1,0:T(8,128)S(1)}, f32[1,1,128,256]{3,2,1,0:T(8,128)}, u32[]{:S(2)}) copy-start(f32[1,1,128,256]{3,2,1,0:T(8,128)} %param.30) | copy-start | bytes 393220
  91.6 2.4 %copy-start.8 = (bf16[128,256]{1,0:T(8,128)(2,1)}, bf16[128,256]{1,0:T(8,128)(2,1)S(1)}, u32[]{:S(2)}) copy-start(bf16[128,256]{1,0:T(8,128)(2,1)S(1)} %convolution_convert_fusion.1) | copy-start | bytes 196612
  116.1 17.7 %copy-start.9 = (bf16[128,256]{1,0:T(8,128)(2,1)S(1)}, bf16[128,256]{1,0:T(8,128)(2,1)}, u32[]{:S(2)}) copy-start(bf16[128,256]{1,0:T(8,128)(2,1)} %copy-done.8) | copy-start | bytes 196612
  116.1 17.7 %copy-start.10 = (bf16[1,128,128]{2,1,0:T(8,128)(2,1)S(1)}, bf16[1,128,128]{2,1,0:T(8,128)(2,1)}, u32[]{:S(2)}) copy-start(bf16[1,128,128]{2,1,0:T(8,128)(2,1)} %param.26) | copy-start | bytes 98308
  116.1 103.0 %all-to-all-start = ((bf16[32,64,256]{2,1,0:T(8,128)(2,1)}), bf16[32,64,256]{2,1,0:T(8,128)(2,1)}, u32[]{:S(2)}, u32[]{:S(2)}) async-start(bf16[32,64,256]{2,1,0:T(8,128)(2,1)} %bitcast.324), calls=%async_computation | async-start | bytes 2097152 | tf_op jit(solution)/shard_map/all_to_all | solution.py:453
  148.5 63.4 %copy-start.7 = (f32[2,1,64,256]{3,2,1,0:T(8,128)S(1)}, f32[2,1,64,256]{3,2,1,0:T(8,128)}, u32[]{:S(2)}) copy-start(f32[2,1,64,256]{3,2,1,0:T(8,128)} %get-tuple-element.524) | copy-start | bytes 393220
  218.5 3.4 %copy-start.11 = (bf16[2,1,64,256]{3,2,1,0:T(8,128)(2,1)}, bf16[2,1,64,256]{3,2,1,0:T(8,128)(2,1)S(1)}, u32[]{:S(2)}) copy-start(bf16[2,1,64,256]{3,2,1,0:T(8,128)(2,1)S(1)} %get-tuple-element.247) | copy-start | bytes 196612

commit v2 on v1

v2 whole, which is shorter than its diff:
```python
import functools

import jax
import jax.numpy as jnp
from jax import lax
from jax.experimental import pallas as pl
from jax.experimental.pallas import tpu as pltpu
from jax.sharding import PartitionSpec as P

X_CHIPS = 4
BF = jnp.bfloat16
F32 = jnp.float32
MSG = 16


def mm(a, b, dims=((1,), (0,))):
    return lax.dot_general(a, b, (dims, ((), ())), preferred_element_type=F32)


def silu_slope_of(v, sig):
    return sig * (1.0 + v * (1.0 - sig))


def kernel(
    sizes,
    x_hbm, g_hbm, routes_ref, rw_ref, wg_hbm, wu_hbm, wd_hbm,
    wo_hbm, q_hbm, k_hbm, v_hbm, decay_ref, state_hbm,
    gg_ref, ug_ref, dg_ref, og_ref, qg_ref, kg_ref, vg_ref,
    xs, gs, wgu, wd, pt, send, recv, rows, acc_gu, acc_hb, gbub, hid,
    part, part_in, out_r, out_l, in_r, in_l, back, ret, mixed,
    wo, qv, kv, vv, st, heads, keep_out, keep_in, carried, pieces_in, pieces_out, s_in,
    mg_out, mg_in, scores_v, acc_hg,
    load_sem, a2a_send, a2a_recv, ag_send, ag_recv, pp_send, pp_recv,
    rs_send, rs_recv, ret_send, ret_recv, mg_send, mg_recv,
    keep_send, keep_recv, hx_send, hx_recv, hz_send, hz_recv,
    sc_send, sc_recv, sb_send, sb_recv, op_send, op_recv,
):
    n_sp, n_tp, n_x, cap, slots = sizes
    n_z = n_sp // n_x
    z_half = n_z // 2
    n_chip = n_tp // 2
    half = n_chip // 2
    tok = x_hbm.shape[0]
    width = xs.shape[1]
    n_rows = n_sp * cap
    hr = n_rows // 2
    s, t = lax.axis_index("sp"), lax.axis_index("tp")
    chip, par = t // 2, t % 2
    partner = t + 1 - 2 * par

    def tp_of(c, parity=None):
        return lax.rem(c + 2 * n_chip, n_chip) * 2 + (par if parity is None else parity)

    right, left = tp_of(chip + 1), tp_of(chip - 1)
    z, x = s // n_x, s % n_x

    def sp_of(zz, xx):
        return lax.rem(zz + n_z, n_z) * n_x + lax.rem(xx + n_x, n_x)

    def remote(src, dst, ssem, rsem, where):
        return pltpu.make_async_remote_copy(
            src_ref=src, dst_ref=dst, send_sem=ssem, recv_sem=rsem,
            device_id=where, device_id_type=pl.DeviceIdType.MESH,
        )

    share = pl.ds(pl.multiple_of(t * width, width), width)
    loads = [
        pltpu.make_async_copy(x_hbm.at[:, share], xs, load_sem.at[0]),
        pltpu.make_async_copy(g_hbm.at[:, share], gs, load_sem.at[1]),
        pltpu.make_async_copy(wg_hbm, wgu.at[:, pl.ds(0, width)], load_sem.at[2]),
        pltpu.make_async_copy(wu_hbm, wgu.at[:, pl.ds(width, width)], load_sem.at[3]),
        pltpu.make_async_copy(wd_hbm, wd, load_sem.at[4]),
        pltpu.make_async_copy(q_hbm, qv, load_sem.at[5]),
        pltpu.make_async_copy(k_hbm, kv, load_sem.at[6]),
        pltpu.make_async_copy(v_hbm, vv, load_sem.at[7]),
        pltpu.make_async_copy(state_hbm, st, load_sem.at[8]),
        pltpu.make_async_copy(wo_hbm, wo, load_sem.at[9]),
    ]
    for c in loads:
        c.start()

    recv[...] = jnp.zeros_like(recv)
    ret[...] = jnp.zeros_like(ret)
    barrier = pltpu.get_barrier_semaphore()

    def greet_sp(d, carry):
        pl.semaphore_signal(
            barrier, inc=1, device_id={"sp": lax.rem(s + d, n_sp), "tp": t},
            device_id_type=pl.DeviceIdType.MESH)
        return carry

    def greet_tp(d, carry):
        pl.semaphore_signal(
            barrier, inc=1, device_id={"sp": s, "tp": tp_of(chip + d)},
            device_id_type=pl.DeviceIdType.MESH)
        return carry

    lax.fori_loop(1, n_sp, greet_sp, 0)
    lax.fori_loop(1, n_chip, greet_tp, 0)
    pl.semaphore_signal(barrier, inc=1, device_id={"sp": s, "tp": partner},
                        device_id_type=pl.DeviceIdType.MESH)

    r0, r1 = routes_ref[0:1, :], routes_ref[1:2, :]
    line = lax.broadcasted_iota(jnp.int32, (n_sp * slots, tok), 0)
    expert, place = line // slots, line % slots
    first, second = r0 == expert, r1 == expert
    named = jnp.where(first | second, 1.0, 0.0)
    row_i = lax.broadcasted_iota(jnp.int32, (tok, tok), 0)
    col_i = lax.broadcasted_iota(jnp.int32, (tok, tok), 1)
    earlier = jnp.where(row_i < col_i, 1.0, 0.0).astype(BF)
    count = mm(named.astype(BF), earlier)
    here = count == place.astype(F32)
    p0 = jnp.where(first & here, 1.0, 0.0).astype(BF)
    p1 = jnp.where(second & here, 1.0, 0.0).astype(BF)
    pt[...] = jnp.where((first | second) & here, 1.0, 0.0).astype(BF)

    def column(row):
        return jnp.sum(jnp.where(row_i == col_i, row, 0.0), axis=1, keepdims=True)

    loads[0].wait()
    loads[1].wait()
    gf = gs[...].astype(F32)
    sg0 = (column(rw_ref[0:1, :]) * gf).astype(BF)
    sg1 = (column(rw_ref[1:2, :]) * gf).astype(BF)
    xv = xs[...]
    sendrows = mm(p0, jnp.concatenate([xv, sg0], axis=1))
    sendrows += mm(p1, jnp.concatenate([xv, sg1], axis=1))
    send[...] = sendrows.astype(BF)

    pl.semaphore_wait(barrier, n_sp - 1 + n_chip - 1 + 1)

    def block(ref, e, length=slots):
        return ref.at[pl.ds(pl.multiple_of(e * slots, slots), length)]

    def dispatch(d, carry):
        e = lax.rem(s + d, n_sp)
        remote(block(send, e, MSG), block(recv, s, MSG), a2a_send.at[e], a2a_recv.at[s],
               {"sp": e, "tp": t}).start()
        return carry

    lax.fori_loop(1, n_sp, dispatch, 0)
    recv[pl.ds(pl.multiple_of(s * slots, slots), slots), :] = send[
        pl.ds(pl.multiple_of(s * slots, slots), slots), :]

    for c in loads[5:9]:
        c.wait()
    decay_col = column(decay_ref[...])
    upto = jnp.where(col_i <= row_i, decay_ref[...], 0.0)
    sum_col = jnp.sum(upto, axis=1, keepdims=True)
    sum_row = jnp.sum(jnp.where(row_i <= col_i, decay_col, 0.0), axis=0, keepdims=True)
    end = jnp.sum(decay_ref[...], axis=1, keepdims=True)
    lower = col_i <= row_i
    table = jnp.where(lower, jnp.exp(jnp.where(lower, sum_col - sum_row, 0.0)), 0.0)
    lead, trail = jnp.exp(sum_col), jnp.exp(end - sum_col)
    keep_out[...] = jnp.broadcast_to(jnp.exp(end), keep_out.shape)
    scale = qv.shape[1] ** -0.5
    q_all, k_all, v_all = qv[...], kv[...], vv[...]
    q_lead = (q_all.astype(F32) * lead).astype(BF)
    scores = (mm(q_all, k_all, ((1,), (1,))) * scale * table).astype(BF)
    scores_v[...] = scores
    state = st[...].astype(BF)
    made = (mm(scores, v_all) + mm(q_lead, state)).astype(BF)
    ht = tok // 2
    mine = pl.ds(pl.multiple_of(s * ht, ht), ht)
    heads[0, mine, :] = made[:ht]
    heads[1, mine, :] = made[ht:]

    def arrived(d, carry):
        e = lax.rem(s + d, n_sp)
        c = remote(block(send, e, MSG), block(recv, e, MSG), a2a_send.at[e], a2a_recv.at[e],
                   {"sp": e, "tp": t})
        c.wait()
        return carry

    lax.fori_loop(1, n_sp, arrived, 0)

    def give_keep(d, carry):
        e = lax.rem(s + d, n_sp)
        remote(keep_out, keep_in.at[s], keep_send.at[e], keep_recv.at[s],
               {"sp": e, "tp": t}).start()
        return carry

    head_copies = []

    def across(h, owner, where, k):
        at = pl.ds(pl.multiple_of(owner * ht, ht), ht)
        return remote(heads.at[h, at], heads.at[h, at], hx_send.at[h, k],
                      hx_recv.at[h, owner % n_x], {"sp": where, "tp": t})

    def along(h, row, where, k):
        at = pl.ds(pl.multiple_of(row * n_x * ht, n_x * ht), n_x * ht)
        return remote(heads.at[h, at], heads.at[h, at], hz_send.at[k], hz_recv.at[h, row],
                      {"sp": where, "tp": t})

    def z_goes(direction, h, k):
        return k < z_half or (k == z_half and h == direction)

    z_sent = [0]

    def z_send(h, row, direction):
        c = along(h, row, sp_of(z + 1 if direction == 0 else z - 1, x), z_sent[0])
        z_sent[0] += 1
        c.start()
        head_copies.append(c)

    def heads_step(k):
        for h in (0, 1):
            if k == 0:
                for d in range(1, n_x):
                    across(h, sp_of(z, x + d), s, d - 1).wait_recv()
                for direction in (0, 1):
                    if z_goes(direction, h, 1):
                        z_send(h, z, direction)
                continue
            for direction in (0, 1):
                if not z_goes(direction, h, k):
                    continue
                row = lax.rem(z - k + n_z if direction == 0 else z + k, n_z)
                along(h, row, s, 0).wait_recv()
                if z_goes(direction, h, k + 1):
                    z_send(h, row, direction)

    dense_r = lax.broadcasted_iota(jnp.int32, (n_rows, n_sp * slots), 0)
    padded_c = lax.broadcasted_iota(jnp.int32, (n_rows, n_sp * slots), 1)
    squeeze = jnp.where(
        padded_c == (dense_r // cap) * slots + dense_r % cap, 1.0, 0.0).astype(BF)
    packed = mm(squeeze, recv[...]).astype(BF)
    rows[t, 0] = packed[:, :width]
    rows[t, 1] = packed[:, width:]

    started = []

    def pass_on(origin, u, where, k):
        c = remote(rows.at[origin, u], rows.at[origin, u], ag_send.at[k], ag_recv.at[origin, u],
                   {"sp": s, "tp": where})
        c.start()
        started.append(c)

    def await_rows(origin, u):
        remote(rows.at[origin, u], rows.at[origin, u], ag_send.at[0], ag_recv.at[origin, u],
               {"sp": s, "tp": partner}).wait_recv()

    n_sent = 0

    def next_sem():
        nonlocal n_sent
        n_sent += 1
        return n_sent - 1

    def goes(direction, u, k):
        return k < half or (k == half and u == direction)

    for u in (0, 1):
        if goes(0, u, 1):
            pass_on(t, u, right, next_sem())
        if goes(1, u, 1):
            pass_on(t, u, left, next_sem())
    for u in (0, 1):
        pass_on(t, u, partner, next_sem())

    for h in (0, 1):
        for d in range(1, n_x):
            c = across(h, s, sp_of(z, x + d), d - 1)
            c.start()
            head_copies.append(c)
    keep_in[s] = keep_out[...]
    lax.fori_loop(1, n_sp, give_keep, 0)
    acc_gu[...] = jnp.zeros_like(acc_gu)
    acc_hb[...] = jnp.zeros_like(acc_hb)
    for c in loads[2:5]:
        c.wait()

    def feats(c):
        return pl.ds(pl.multiple_of(c * 2 * width, 2 * width), 2 * width)

    def forward(c):
        for u in (0, 1):
            await_rows(tp_of(c, 1 - par), u)
        xin = jnp.concatenate([rows[2 * c, 0], rows[2 * c + 1, 0]], axis=1)
        gin = jnp.concatenate([rows[2 * c, 1], rows[2 * c + 1, 1]], axis=1)
        acc_gu[...] += mm(xin, wgu[feats(c), :])
        acc_hb[...] += mm(gin, wd[:, feats(c)], ((1,), (1,)))

    ready = [chip]
    for k in range(1, half + 1):
        from_left, from_right = lax.rem(chip - k + n_chip, n_chip), lax.rem(chip + k, n_chip)
        for u in (0, 1):
            if goes(0, u, k):
                o = from_left * 2 + par
                await_rows(o, u)
                if goes(0, u, k + 1):
                    pass_on(o, u, right, next_sem())
                pass_on(o, u, partner, next_sem())
            if goes(1, u, k):
                o = from_right * 2 + par
                await_rows(o, u)
                if goes(1, u, k + 1):
                    pass_on(o, u, left, next_sem())
                pass_on(o, u, partner, next_sem())
        for c in ready:
            forward(c)
        if k - 1 <= z_half:
            heads_step(k - 1)
        ready = [from_left, from_right] if k < half else [from_left]
    for c in ready:
        forward(c)
    for c in started:
        c.wait_send()

    gate_pre, up_pre = acc_gu[:, :width], acc_gu[:, width:]
    sig = jax.nn.sigmoid(gate_pre)
    active = gate_pre * sig
    hb = acc_hb[...]
    hid[...] = (active * up_pre).astype(BF)
    gbub[:, :width] = (hb * up_pre * silu_slope_of(gate_pre, sig)).astype(BF)
    gbub[:, width:] = (hb * active).astype(BF)

    order = [chip + half]
    for k in range(half - 1, 0, -1):
        order += [chip + k, chip - k]
    order = [lax.rem(c + n_chip, n_chip) for c in order + [chip]]
    shared = []
    gb_all = gbub[...]
    for n, c in enumerate(order):
        value = mm(gb_all, wgu[feats(c), :], ((1,), (1,))).astype(BF)
        part[c, 0] = value[:, :width]
        part[c, 1] = value[:, width:]
        cp = remote(part.at[c, 1 - par], part_in.at[c], pp_send.at[n], pp_recv.at[c],
                    {"sp": s, "tp": partner})
        cp.start()
        shared.append(cp)

    def await_part(c):
        remote(part.at[c, 1 - par], part_in.at[c], pp_send.at[0], pp_recv.at[c],
               {"sp": s, "tp": partner}).wait_recv()

    cut = (pl.ds(0, hr), pl.ds(hr, hr))
    sums = []

    def ring_copy(direction, i, h):
        out, inn = (out_r, in_r) if direction == 0 else (out_l, in_l)
        return remote(out.at[i - 1, cut[h]], inn.at[i - 1, cut[h]],
                      rs_send.at[direction, i - 1, h], rs_recv.at[direction, i - 1, h],
                      {"sp": s, "tp": right if direction == 0 else left})

    def has(direction, i, h):
        return i >= 2 or h == direction

    for i in range(1, half + 1):
        d = half + 1 - i
        targets = (lax.rem(chip + d, n_chip), lax.rem(chip - d + n_chip, n_chip))
        if i == 1:
            await_part(targets[0])
        else:
            await_part(targets[0])
            await_part(targets[1])
        for h in (0, 1):
            for direction in (0, 1):
                if not has(direction, i, h):
                    continue
                out, inn = (out_r, in_r) if direction == 0 else (out_l, in_l)
                c = targets[direction]
                total = part[c, par, cut[h], :].astype(F32) + part_in[c, cut[h], :].astype(F32)
                if i >= 2 and has(direction, i - 1, h):
                    ring_copy(direction, i - 1, h).wait_recv()
                    total += inn[i - 2, cut[h], :].astype(F32)
                out[i - 1, cut[h], :] = total.astype(BF)
                cp = ring_copy(direction, i, h)
                cp.start()
                sums.append(cp)
    for k in range(half, z_half + 1):
        heads_step(k)
    await_part(chip)
    pieces = []
    for h in (0, 1):
        total = part[chip, par, cut[h], :].astype(F32) + part_in[chip, cut[h], :].astype(F32)
        for direction in (0, 1):
            if has(direction, half, h):
                ring_copy(direction, half, h).wait_recv()
                inn = in_r if direction == 0 else in_l
                total += inn[half - 1, cut[h], :].astype(F32)
        pieces.append(total.astype(BF))
    summed = jnp.concatenate(pieces, axis=0)

    padded_r = lax.broadcasted_iota(jnp.int32, (n_sp * slots, n_rows), 0)
    dense_c = lax.broadcasted_iota(jnp.int32, (n_sp * slots, n_rows), 1)
    spread = jnp.where(
        padded_r == (dense_c // cap) * slots + dense_c % cap, 1.0, 0.0).astype(BF)
    back[...] = mm(spread, summed).astype(BF)

    def send_back(d, carry):
        e = lax.rem(s + d, n_sp)
        remote(block(back, e, MSG), block(ret, s, MSG), ret_send.at[e], ret_recv.at[s],
               {"sp": e, "tp": t}).start()
        return carry

    lax.fori_loop(1, n_sp, send_back, 0)
    ret[pl.ds(pl.multiple_of(s * slots, slots), slots), :] = back[
        pl.ds(pl.multiple_of(s * slots, slots), slots), :]

    hid_all = hid[...]
    for c in range(n_chip):
        xin = jnp.concatenate([rows[2 * c, 0], rows[2 * c + 1, 0]], axis=1)
        gin = jnp.concatenate([rows[2 * c, 1], rows[2 * c + 1, 1]], axis=1)
        both = mm(xin, gb_all, ((0,), (0,)))
        at = pl.ds(c * 2 * width, 2 * width)
        gg_ref[at, :] = both[:, :width].astype(BF)
        ug_ref[at, :] = both[:, width:].astype(BF)
        dg_ref[:, at] = mm(hid_all, gin, ((0,), (0,))).astype(BF)
    for cp in shared + sums:
        cp.wait_send()

    def returned(d, carry):
        e = lax.rem(s + d, n_sp)
        remote(block(back, e, MSG), block(ret, e, MSG), ret_send.at[e], ret_recv.at[e],
               {"sp": e, "tp": t}).wait()
        return carry

    lax.fori_loop(1, n_sp, returned, 0)
    mixed[t] = (gs[...].astype(F32) + mm(pt[...], ret[...], ((0,), (0,)))).astype(BF)

    def mixed_copy(origin, where, k):
        return remote(mixed.at[origin], mixed.at[origin], mg_send.at[k], mg_recv.at[origin],
                      {"sp": s, "tp": where})

    copies = []
    for d in range(half, 0, -1):
        for c in sorted({d, n_chip - d}):
            cp = mixed_copy(t, tp_of(chip + c), c)
            cp.start()
            copies.append(cp)
    cp = mixed_copy(t, partner, 0)
    cp.start()
    copies.append(cp)
    for d in range(1, half + 1):
        for c in sorted({d, n_chip - d}):
            o = tp_of(chip + c)
            mixed_copy(o, partner, n_chip + c).wait_recv()
            cp = mixed_copy(o, partner, n_chip + c)
            cp.start()
            copies.append(cp)
    loads[9].wait()
    acc_hg[...] = jnp.zeros_like(acc_hg)
    for d in range(half + 1):
        for c in sorted({d, (n_chip - d) % n_chip}):
            o = lax.rem(chip + c, n_chip)
            mixed_copy(o * 2 + 1 - par, partner, 0).wait_recv()
            acc_hg[...] += mm(jnp.concatenate([mixed[2 * o], mixed[2 * o + 1]], axis=1), wo[feats(o), :])

    hg = acc_hg[...].astype(BF)
    carried[...] = mm(q_lead, hg, ((0,), (0,)))
    pr = pieces_in.shape[1]

    def piece(ref, i):
        return ref.at[pl.ds(pl.multiple_of((i // 2) * pr, 8), pr),
                      pl.ds(pl.multiple_of((i % 2) * 128, 128), 128)]

    def give_piece(d, carry):
        e = lax.rem(s + d, n_sp)
        remote(piece(carried, e), pieces_in.at[s], sc_send.at[e], sc_recv.at[s],
               {"sp": e, "tp": t}).start()
        return carry

    lax.fori_loop(1, n_sp, give_piece, 0)
    pieces_in[s] = piece(carried, s)[...]
    back_scores = (mm(hg, v_all, ((1,), (1,))) * table).astype(BF)
    hg_lead = (acc_hg[...].astype(BF).astype(F32) * lead).astype(BF)

    lane = lax.broadcasted_iota(jnp.int32, (ht, width), 1)
    for o in range(n_tp):
        both = mixed[o].astype(F32)
        top, bottom = both[:ht], both[ht:]
        mg_out[2 * o] = jnp.where(lane < 64, top, pltpu.roll(bottom, 64, 1)).astype(BF)
        mg_out[2 * o + 1] = jnp.where(lane < 64, pltpu.roll(top, 64, 1), bottom).astype(BF)

    def mg_piece(e):
        return mg_in.at[pl.ds(pl.multiple_of(e * ht, ht), ht)]

    def give_mg(d, carry):
        e = lax.rem(s + d, n_sp)
        remote(mg_out.at[e], mg_piece(s), op_send.at[e], op_recv.at[s], {"sp": e, "tp": t}).start()
        return carry

    lax.fori_loop(1, n_sp, give_mg, 0)
    mg_in[mine, :] = mg_out[s]

    qg_ref[...] = (mm(back_scores, k_all) * scale + mm(hg_lead, state, ((1,), (1,)))).astype(BF)
    key_part = mm(back_scores, q_all, ((0,), (0,)))
    value_part = mm(scores_v[...], hg, ((0,), (0,)))

    def keep_here(d, carry):
        e = lax.rem(s + d, n_sp)
        remote(keep_out, keep_in.at[e], keep_send.at[e], keep_recv.at[e], {"sp": e, "tp": t}).wait()
        return carry

    lax.fori_loop(1, n_sp, keep_here, 0)

    def piece_here(d, carry):
        e = lax.rem(s + d, n_sp)
        remote(piece(carried, e), pieces_in.at[e], sc_send.at[e], sc_recv.at[e],
               {"sp": e, "tp": t}).wait()
        return carry

    lax.fori_loop(1, n_sp, piece_here, 0)
    running = jnp.zeros(pieces_in.shape[1:], F32)
    for p in range(n_sp - 1, -1, -1):
        pieces_out[p] = running
        running = pieces_in[p] + keep_in[p][0:1, :] * running

    def give_state(d, carry):
        e = lax.rem(s + d, n_sp)
        remote(pieces_out.at[e], piece(s_in, s), sb_send.at[e], sb_recv.at[s],
               {"sp": e, "tp": t}).start()
        return carry

    lax.fori_loop(1, n_sp, give_state, 0)
    piece(s_in, s)[...] = pieces_out[s]

    def mg_here(d, carry):
        e = lax.rem(s + d, n_sp)
        remote(mg_out.at[e], mg_piece(e), op_send.at[e], op_recv.at[e], {"sp": e, "tp": t}).wait()
        return carry

    lax.fori_loop(1, n_sp, mg_here, 0)
    slices = mg_in[...]
    og_ref[...] = (mm(slices, heads[0], ((0,), (0,)))[: width // 2]
                   + mm(slices, heads[1], ((0,), (0,)))[width // 2:])

    def state_here(d, carry):
        e = lax.rem(s + d, n_sp)
        remote(pieces_out.at[e], piece(s_in, e), sb_send.at[e], sb_recv.at[e],
               {"sp": e, "tp": t}).wait()
        return carry

    lax.fori_loop(1, n_sp, state_here, 0)
    later = s_in[...].astype(BF)
    v_trail = (v_all.astype(F32) * trail).astype(BF)
    k_trail = (k_all.astype(F32) * (scale * trail)).astype(BF)
    kg_ref[...] = ((key_part + mm(v_trail, later, ((1,), (1,)))) * scale).astype(BF)
    vg_ref[...] = (value_part + mm(k_trail, later)).astype(BF)
    for cp in copies + head_copies:
        cp.wait_send()


def program(sizes, moe_input, out_grad, routes, route_weight, w_gate, w_up, w_down,
            w_out, query, key, value, log_decay, state_in):
    n_sp, n_tp, n_x = sizes
    tok, model = moe_input.shape
    cap = 5 * tok * routes.shape[0] // (4 * n_sp)
    slots = -(-cap // 16) * 16
    width = model // n_tp
    hidden = w_gate.shape[1]
    n_rows = n_sp * cap
    n_chip = n_tp // 2
    half = n_chip // 2
    n_z = n_sp // n_x
    dk, dv = query.shape[1], value.shape[1]
    pr = dk * dv // (128 * n_sp)
    hbm = pl.BlockSpec(memory_space=pltpu.HBM)
    vmem = pl.BlockSpec(memory_space=pltpu.VMEM)
    dma = pltpu.SemaphoreType.DMA
    n_ag = 2 * (2 * half - 1) + 2 * n_chip
    return pl.pallas_call(
        functools.partial(kernel, (n_sp, n_tp, n_x, cap, slots)),
        name="whole",
        out_shape=(
            jax.ShapeDtypeStruct((model, hidden), BF),
            jax.ShapeDtypeStruct((model, hidden), BF),
            jax.ShapeDtypeStruct((hidden, model), BF),
            jax.ShapeDtypeStruct((model // n_sp, dv), F32),
            jax.ShapeDtypeStruct((tok, dk), BF),
            jax.ShapeDtypeStruct((tok, dk), BF),
            jax.ShapeDtypeStruct((tok, dv), BF),
        ),
        in_specs=[hbm, hbm, vmem, vmem, hbm, hbm, hbm, hbm, hbm, hbm, hbm, vmem, hbm],
        out_specs=(vmem,) * 7,
        scratch_shapes=[
            pltpu.VMEM((tok, width), BF),
            pltpu.VMEM((tok, width), BF),
            pltpu.VMEM((model, 2 * hidden), BF),
            pltpu.VMEM((hidden, model), BF),
            pltpu.VMEM((n_sp * slots, tok), BF),
            pltpu.VMEM((n_sp * slots, 2 * width), BF),
            pltpu.VMEM((n_sp * slots, 2 * width), BF),
            pltpu.VMEM((n_tp, 2, n_rows, width), BF),
            pltpu.VMEM((n_rows, 2 * hidden), F32),
            pltpu.VMEM((n_rows, hidden), F32),
            pltpu.VMEM((n_rows, 2 * hidden), BF),
            pltpu.VMEM((n_rows, hidden), BF),
            pltpu.VMEM((n_chip, 2, n_rows, width), BF),
            pltpu.VMEM((n_chip, n_rows, width), BF),
            pltpu.VMEM((half, n_rows, width), BF),
            pltpu.VMEM((half, n_rows, width), BF),
            pltpu.VMEM((half, n_rows, width), BF),
            pltpu.VMEM((half, n_rows, width), BF),
            pltpu.VMEM((n_sp * slots, width), BF),
            pltpu.VMEM((n_sp * slots, width), BF),
            pltpu.VMEM((n_tp, tok, width), BF),
            pltpu.VMEM((model, dv), BF),
            pltpu.VMEM((tok, dk), BF),
            pltpu.VMEM((tok, dk), BF),
            pltpu.VMEM((tok, dv), BF),
            pltpu.VMEM((dk, dv), F32),
            pltpu.VMEM((2, n_sp * tok // 2, dv), BF),
            pltpu.VMEM((8, 128), F32),
            pltpu.VMEM((n_sp, 8, 128), F32),
            pltpu.VMEM((dk, dv), F32),
            pltpu.VMEM((n_sp, pr, 128), F32),
            pltpu.VMEM((n_sp, pr, 128), F32),
            pltpu.VMEM((dk, dv), F32),
            pltpu.VMEM((n_sp, tok // 2, width), BF),
            pltpu.VMEM((n_sp * tok // 2, width), BF),
            pltpu.VMEM((tok, tok), BF),
            pltpu.VMEM((tok, dv), F32),
            dma((10,)),
            dma((n_sp,)),
            dma((n_sp,)),
            dma((n_ag,)),
            dma((n_tp, 2)),
            dma((n_chip + 1,)),
            dma((n_chip,)),
            dma((2, half, 2)),
            dma((2, half, 2)),
            dma((n_sp,)),
            dma((n_sp,)),
            dma((2 * n_chip,)),
            dma((n_tp,)),
            dma((n_sp,)),
            dma((n_sp,)),
            dma((2, n_x)),
            dma((2, n_x)),
            dma((2 * n_z,)),
            dma((2, n_z)),
            dma((n_sp,)),
            dma((n_sp,)),
            dma((n_sp,)),
            dma((n_sp,)),
            dma((n_sp,)),
            dma((n_sp,)),
        ],
        compiler_params=pltpu.CompilerParams(
            collective_id=0, has_side_effects=True, vmem_limit_bytes=60 << 20
        ),
    )(moe_input, out_grad, routes, route_weight, w_gate, w_up, w_down,
      w_out, query, key, value, log_decay, state_in)


def solution(mesh):
    sizes = (mesh.shape["sp"], mesh.shape["tp"], X_CHIPS)

    def body(moe_input, out_grad, routes, route_weight, w_gate, w_up, w_down,
             w_out, query, key, value, log_decay, state_in):
        gate, up, down, proj, dq, dk, dv = program(
            sizes, moe_input, out_grad, routes.T, route_weight.T, w_gate[0], w_up[0], w_down[0],
            w_out, query[0], key[0], value[0], log_decay, state_in[0, 0])
        return gate[None], up[None], down[None], proj, dq[None], dk[None], dv[None]

    rows, heads = P("sp", None), P("tp", "sp", None)
    columns, lines = P("sp", None, "tp"), P("sp", "tp", None)
    return jax.shard_map(
        body,
        mesh=mesh,
        in_specs=(rows, rows, rows, rows, columns, columns, lines, P(None, "tp"),
                  heads, heads, heads, P("tp", "sp"), P("tp", "sp", None, None)),
        out_specs=(columns, columns, lines, P("sp", "tp"), heads, heads, heads),
        check_vma=False,
    )
```

time: 225 us -> 118 us (0.52)
  the two profiles are of different devices: /device:TPU:8 before, /device:TPU:1 now
where the time goes in v2:
time: 118 us
  Pallas kernels  111 us (94%)
  local copies, waits for them, and re-layouts  6.64 us (6%)
    pallas_call x1, Pallas kernels, program(): pl.pallas_call(functools.partial(kernel, (n_sp, n_tp, n_x, cap, slots)),...  111 us
    unnamed x19, local copies, waits for them, and re-layouts  6.64 us

profile of v2, /device:TPU:1, one launch (start us, length us, event | category | flops | bytes accessed | tf_op | source)
XLA Modules:
  0.0 118.0 jit_solution(1539379111081870357)
XLA Ops:
  0.6 110.7 %whole.1 = (bf16[2048,128]{1,0:T(8,128)(2,1)}, bf16[2048,128]{1,0:T(8,128)(2,1)}, bf16[128,2048]{1,0:T(8,128)(2,1)}, f32[64,256]{1,0:T(8,128)}, bf16[128,128]{1,...) custom-call(bf16[128,2048]{1,0:T(8,128)(2,1)} %x_hbm.1, bf16[128,2048]{1,0:T(8,128)(2,1)} %g_hbm.1, ...), custom_call_target="tpu_custom_call" | custom-call | tf_op jit(solution)/shard_map/whole/pallas_call | solution.py:563
  111.4 0.0 copy-start.1
  111.4 1.9 %copy.27 = bf16[1,2048,128]{2,1,0:T(8,128)(2,1)} copy(bf16[1,2048,128]{2,1,0:T(8,128)(2,1)} %bitcast.17) | data formatting | bytes 1048576
  113.3 0.0 copy-done.1
  113.3 0.0 copy-start
  113.3 0.8 copy.28
  114.1 0.4 copy-done
  114.5 0.0 copy-start.3
  114.5 0.8 copy.29
  115.3 0.1 copy-done.3
  115.4 0.0 copy-start.5
  115.4 0.0 copy-start.4
  115.4 0.6 copy.30
  116.0 0.1 copy-done.5
  116.2 0.0 copy-start.2
  116.2 0.6 copy.31
  116.8 0.0 copy-done.4
  116.8 0.6 copy.32
  117.4 0.0 copy-done.2
  117.4 0.6 copy.33
Async XLA Ops:
  111.4 1.9 %copy-start.1 = (bf16[2048,128]{1,0:T(8,128)(2,1)S(1)}, bf16[2048,128]{1,0:T(8,128)(2,1)}, u32[]{:S(2)}) copy-start(bf16[2048,128]{1,0:T(8,128)(2,1)} %get-tuple-element.15) | copy-start | bytes 1572868
  113.3 1.2 %copy-start = (bf16[128,2048]{1,0:T(8,128)(2,1)S(1)}, bf16[128,2048]{1,0:T(8,128)(2,1)}, u32[]{:S(2)}) copy-start(bf16[128,2048]{1,0:T(8,128)(2,1)} %get-tuple-element.16) | copy-start | bytes 1572868
  114.5 0.9 copy-start.3
  115.4 0.8 copy-start.5
  115.4 1.4 %copy-start.4 = (bf16[128,128]{1,0:T(8,128)(2,1)S(1)}, bf16[128,128]{1,0:T(8,128)(2,1)}, u32[]{:S(2)}) copy-start(bf16[128,128]{1,0:T(8,128)(2,1)} %get-tuple-element.19) | copy-start | bytes 98308
  116.2 1.2 %copy-start.2 = (bf16[128,256]{1,0:T(8,128)(2,1)S(1)}, bf16[128,256]{1,0:T(8,128)(2,1)}, u32[]{:S(2)}) copy-start(bf16[128,256]{1,0:T(8,128)(2,1)} %get-tuple-element.20) | copy-start | bytes 196612
